TPU v7x, 32 devices: a whole 2x2x4 slice. The times are simulated.
32 devices in a mesh: row: 8 (over z, core), col: 4 (over y, x).
Axes of the slice: x: 2, y: 2, z: 4, core: 2. Of those that a mesh axis runs over, the one named last changes fastest.
Arguments:
- tokens: bfloat16 [1, 2048, 2048], P(None, 'row'), may hold values from -6 to 6
- w_value: bfloat16 [2048, 1024], P(None, 'col'), may hold values from -0.125 to 0.125
- w_first: bfloat16 [2048, 1024], P(None, 'col'), may hold values from -0.125 to 0.125
- w_second: bfloat16 [2048, 1024], P(None, 'col'), may hold values from -0.125 to 0.125
- w_gate: bfloat16 [2048, 1024], P(None, 'col'), may hold values from -0.125 to 0.125
- conv_taps: float32 [3, 3, 1024], P(None, None, 'col'), may hold values from -3.5 to 3.5
- filter_embed: float32 [33, 64], replicated, may hold values from -48 to 48
- filter_freq: float32 [64], replicated, may hold values from 0.1 to 1.9
- filter_proj: float32 [64, 2, 2, 1024], P(None, None, None, 'col'), may hold values from -0.0234375 to 0.0234375
- filter_decay: float32 [2, 2, 1024], P(None, None, 'col'), may hold values from 0.25 to 32
- skip_gain: float32 [2, 1024], P(None, 'col'), may hold values from -3 to 3
- w_out: bfloat16 [1024, 2048], P('col'), may hold values from -0.1875 to 0.1875
Outputs:
- mixed: bfloat16 [1, 2048, 2048], P(None, ('row', 'col'))
All inputs are finite; a program needn't handle non-finite values.
Results may differ from a plain program's by a relative error of at most 0.018.
Values may be sent and summed in bfloat16 or wider, within the bound.
A program may use at most 64 MiB of HBM per device.

v0:
```python
import functools
import math

import jax
import jax.numpy as jnp
import numpy as np
from jax import lax
from jax.experimental import pallas as pl
from jax.experimental.pallas import tpu as pltpu
from jax.sharding import PartitionSpec as P

precise = lax.Precision.HIGHEST


def padded_2(array, sides, width):
    for axis, dim in sides:
        size, length = (lax.axis_size(axis), array.shape[dim])
        up = [(i, (i + 1) % size) for i in range(size - 1)]
        down = [(j, i) for i, j in up]
        last = lax.slice_in_dim(array, length - width, length, axis=dim)
        leading = lax.slice_in_dim(array, 0, width, axis=dim)
        before = lax.ppermute(last, axis, up)
        after = lax.ppermute(leading, axis, down)
        array = jnp.concatenate([before, array, after], axis=dim)
    return array


def split_length(total):
    factor = math.isqrt(total)
    while total % factor != 0:
        factor = factor - 1
    return (factor, total // factor)


def tables(outer, inner, total):
    first_index = jnp.arange(outer, dtype=jnp.int32)
    second_index = jnp.arange(inner, dtype=jnp.int32)
    scale = 2.0 * math.pi
    outer_angle = (first_index[:, None] * first_index[None, :] % outer).astype(jnp.float32) * (
        scale / outer
    )
    inner_angle = (second_index[:, None] * second_index[None, :] % inner).astype(jnp.float32) * (
        scale / inner
    )
    twist_angle = (first_index[:, None] * second_index[None, :] % total).astype(jnp.float32) * (
        scale / total
    )
    return (
        jnp.cos(outer_angle),
        jnp.sin(outer_angle),
        jnp.cos(inner_angle),
        jnp.sin(inner_angle),
        jnp.cos(twist_angle),
        jnp.sin(twist_angle),
    )


def forward_real(signal, table):
    outer_cos, outer_sin, inner_cos, inner_sin, twist_cos, twist_sin = table
    outer = outer_cos.shape[0]
    inner = inner_cos.shape[0]
    grid = signal.reshape(signal.shape[0], outer, inner)
    real_part = jnp.einsum("kq,cqp->ckp", outer_cos, grid, precision=precise)
    imag_part = -jnp.einsum("kq,cqp->ckp", outer_sin, grid, precision=precise)
    turned_real = real_part * twist_cos + imag_part * twist_sin
    turned_imag = imag_part * twist_cos - real_part * twist_sin
    spec_real = jnp.einsum("ckp,pj->ckj", turned_real, inner_cos, precision=precise) + jnp.einsum(
        "ckp,pj->ckj", turned_imag, inner_sin, precision=precise
    )
    spec_imag = jnp.einsum("ckp,pj->ckj", turned_imag, inner_cos, precision=precise) - jnp.einsum(
        "ckp,pj->ckj", turned_real, inner_sin, precision=precise
    )
    return (spec_real, spec_imag)


def inverse_real(spec_real, spec_imag, table):
    outer_cos, outer_sin, inner_cos, inner_sin, twist_cos, twist_sin = table
    total = outer_cos.shape[0] * inner_cos.shape[0]
    back_real = jnp.einsum("ckj,jp->ckp", spec_real, inner_cos, precision=precise) - jnp.einsum(
        "ckj,jp->ckp", spec_imag, inner_sin, precision=precise
    )
    back_imag = jnp.einsum("ckj,jp->ckp", spec_real, inner_sin, precision=precise) + jnp.einsum(
        "ckj,jp->ckp", spec_imag, inner_cos, precision=precise
    )
    turned_real = back_real * twist_cos - back_imag * twist_sin
    turned_imag = back_real * twist_sin + back_imag * twist_cos
    result = jnp.einsum("qk,ckp->cqp", outer_cos, turned_real, precision=precise) - jnp.einsum(
        "qk,ckp->cqp", outer_sin, turned_imag, precision=precise
    )
    return result.reshape(result.shape[0], total) / total


def channel_filters(
    length, row_index, chan_row, filter_embed, filter_freq, filter_proj, filter_decay
):
    bands = (filter_embed.shape[0] - 1) // 2
    index = jnp.arange(length, dtype=jnp.int32)
    spot = index.astype(jnp.float32) / (length - 1)
    freqs = jnp.arange(1, bands + 1, dtype=jnp.int32)
    phase = (index[:, None] * freqs[None, :] % length).astype(jnp.float32) * (
        2.0 * math.pi / length
    )
    features = jnp.concatenate([spot[:, None], jnp.cos(phase), jnp.sin(phase)], axis=1)
    hidden = jnp.sin(filter_freq[None, :] * jnp.dot(features, filter_embed, precision=precise))
    own_proj = lax.dynamic_slice_in_dim(filter_proj, row_index * chan_row, chan_row, 3)
    own_decay = lax.dynamic_slice_in_dim(filter_decay, row_index * chan_row, chan_row, 2)
    taps = jnp.dot(hidden, own_proj.reshape(own_proj.shape[0], 4 * chan_row), precision=precise)
    taps = jnp.transpose(taps).reshape(2, 2, chan_row, length)
    taps = taps * jnp.exp(-spot[None, None, None, :] * own_decay[:, :, :, None])
    cycles = []
    for order in range(2):
        behind = jnp.flip(taps[order, 1, :, 1:], axis=1)
        cycles.append(
            jnp.concatenate([taps[order, 0], jnp.zeros((chan_row, 1), jnp.float32), behind], axis=1)
        )
    return cycles


def body(
    tokens,
    w_value,
    w_first,
    w_second,
    w_gate,
    conv_taps,
    filter_embed,
    filter_freq,
    filter_proj,
    filter_decay,
    skip_gain,
    w_out,
):
    seq_count = tokens.shape[0]
    tok_rows = tokens.shape[1]
    chan_col = w_value.shape[1]
    row_count = lax.axis_size("row")
    chan_row = chan_col // row_count
    length = tok_rows * row_count
    row_index = lax.axis_index("row")
    proj = jnp.concatenate(
        [
            jnp.dot(tokens, w_value, preferred_element_type=jnp.float32),
            jnp.dot(tokens, w_first, preferred_element_type=jnp.float32),
            jnp.dot(tokens, w_second, preferred_element_type=jnp.float32),
        ],
        axis=2,
    ).astype(jnp.bfloat16)
    gate = jnp.dot(tokens, w_gate, preferred_element_type=jnp.float32).astype(jnp.bfloat16)
    padded = padded_2(proj, (("row", 1),), 1).astype(jnp.float32)
    weights = conv_taps.reshape(3, 3 * chan_col)
    short = padded[:, :-2] * weights[0] + padded[:, 1:-1] * weights[1] + padded[:, 2:] * weights[2]
    value_rows = jnp.transpose(short[:, :, :chan_col], (0, 2, 1))
    first_rows = jnp.transpose(short[:, :, chan_col : 2 * chan_col], (0, 2, 1))
    second_rows = jnp.transpose(short[:, :, 2 * chan_col :], (0, 2, 1))
    outer, inner = split_length(2 * length)
    table = tables(outer, inner, 2 * length)
    cycles = channel_filters(
        length, row_index, chan_row, filter_embed, filter_freq, filter_proj, filter_decay
    )
    spectra = [forward_real(cycle, table) for cycle in cycles]
    own_gain = lax.dynamic_slice_in_dim(skip_gain, row_index * chan_row, chan_row, 1)

    def convolve(signal, order):
        flat = signal.reshape(seq_count * chan_row, length)
        padded_signal = jnp.concatenate([flat, jnp.zeros_like(flat)], axis=1)
        sig_real, sig_imag = forward_real(padded_signal, table)
        sig_real = sig_real.reshape(seq_count, chan_row, outer, inner)
        sig_imag = sig_imag.reshape(seq_count, chan_row, outer, inner)
        filt_real, filt_imag = spectra[order]
        prod_real = sig_real * filt_real[None] - sig_imag * filt_imag[None]
        prod_imag = sig_real * filt_imag[None] + sig_imag * filt_real[None]
        result = inverse_real(
            prod_real.reshape(seq_count * chan_row, outer, inner),
            prod_imag.reshape(seq_count * chan_row, outer, inner),
            table,
        )[:, :length]
        return result.reshape(seq_count, chan_row, length) + own_gain[order][None, :, None] * signal

    value_chan, first_chan = (
        lax.all_to_all(value_rows, "row", split_axis=1, concat_axis=2, tiled=True),
        lax.all_to_all(first_rows, "row", split_axis=1, concat_axis=2, tiled=True),
    )
    inner_chan = first_chan * convolve(value_chan, 0)
    second_conv = lax.all_to_all(
        convolve(inner_chan, 1), "row", split_axis=2, concat_axis=1, tiled=True
    )
    outer_rows = (
        jnp.transpose(second_rows * second_conv, (0, 2, 1)) * jax.nn.silu(gate.astype(jnp.float32))
    ).astype(jnp.bfloat16)
    own_rows = tok_rows // lax.axis_size("col")
    flat_rows = jnp.transpose(outer_rows, (1, 0, 2)).reshape(tok_rows * seq_count, chan_col)
    summed = lax.psum_scatter(
        jnp.dot(flat_rows, w_out, preferred_element_type=jnp.float32).astype(jnp.bfloat16),
        "col",
        scatter_dimension=0,
        tiled=True,
    ).astype(jnp.float32)
    summed = jnp.transpose(summed.reshape(own_rows, seq_count, w_out.shape[1]), (1, 0, 2))
    return summed.astype(jnp.bfloat16)


LANES = 128


def dft_tables(length, chans):
    filled = length // LANES
    outer = 2 * filled
    total = outer * LANES
    half = outer // 2 + 1
    eye = np.eye(chans)
    q, k, p = np.arange(filled), np.arange(half), np.arange(LANES)
    angle = 2.0 * np.pi * (np.outer(k, q) % outer) / outer
    first = np.concatenate([np.kron(np.cos(angle), eye), np.kron(-np.sin(angle), eye)], axis=0)
    weight = np.where((k == 0) | (k == outer // 2), 1.0, 2.0) / total
    last = np.concatenate(
        [np.kron(np.cos(angle).T * weight, eye), np.kron(-np.sin(angle).T * weight, eye)], axis=1
    )
    turn = 2.0 * np.pi * np.outer(k, p) / total
    twist = np.stack([np.cos(turn), np.sin(turn)])[:, :, None, :]
    angle = 2.0 * np.pi * (np.outer(p, p) % LANES) / LANES
    cos, sin = np.cos(angle), np.sin(angle)
    ahead = np.block([[cos, -sin], [sin, cos]])
    back = np.block([[cos, sin], [-sin, cos]])
    low = lambda array: jnp.asarray(array.astype(np.float32)).astype(jnp.bfloat16)
    return low(first), low(last), jnp.asarray(twist.astype(np.float32)), low(ahead), low(back)


def mixer_kernel(
    rows, cols, chans, width, tokens_ref, w_value_ref, w_first_ref, w_second_ref, w_gate_ref, w_out_ref,
    features_ref, embed_ref, own_proj_ref, decay_ref, gains_ref, first_ref, last_ref, small_twist_ref, ahead_ref, back_ref,
    out_ref, proj_ref, recv, sent, recv_rows, recv_cols, spectra, twist_ref, weights, turned_rows, taps_ref,
    value_send, value_recv, rest_send, rest_recv, rows_send, rows_recv, cols_send, cols_recv, own_sem,
    weight_send, weight_recv, relay_send, relay_recv, weight_sem,
):
    my_row = lax.axis_index("row")
    my_col = lax.axis_index("col")
    mesh_id = pl.DeviceIdType.MESH
    length_q = recv.shape[0] * recv.shape[2] // chans
    block_q = recv.shape[2] // chans
    near = 2 if cols % 2 == 0 else 1
    far = cols // near
    side = lax.rem(my_row, 2)
    partner = my_row + 1 - 2 * side
    half_rows = weights.shape[1] // 2

    def col_peer(d):
        return (
            lax.rem(my_col // near + d // near, far) * near
            + lax.rem(lax.rem(my_col, near) + d % near, near)
        )

    barrier = pltpu.get_barrier_semaphore()
    for d in range(1, rows):
        pl.semaphore_signal(
            barrier, inc=1, device_id=(lax.rem(my_row + d, rows), my_col), device_id_type=mesh_id
        )
    for d in range(1, cols):
        pl.semaphore_signal(
            barrier, inc=1, device_id=(my_row, col_peer(d)), device_id_type=mesh_id
        )
    pl.semaphore_wait(barrier, rows + cols - 2)

    def row_copies(part, send_sem, recv_sem):
        copies = []
        for d in range(1, rows):
            peer = lax.rem(my_row + d, rows)
            copies.append(
                pltpu.make_async_remote_copy(
                    src_ref=proj_ref.at[peer, part],
                    dst_ref=recv.at[my_row, part],
                    send_sem=send_sem.at[d - 1],
                    recv_sem=recv_sem.at[d - 1],
                    device_id=(peer, my_col),
                    device_id_type=mesh_id,
                )
            )
        return copies

    own_half = pl.ds(pl.multiple_of(side * half_rows, half_rows), half_rows)
    weight_copies, relays = [], []
    for d in range(1, cols):
        weight_copies.append(
            pltpu.make_async_remote_copy(
                src_ref=w_out_ref.at[own_half],
                dst_ref=weights.at[d, own_half],
                send_sem=weight_send.at[d - 1],
                recv_sem=weight_recv.at[d - 1],
                device_id=(my_row, col_peer(d)),
                device_id_type=mesh_id,
            )
        )
        relays.append(
            pltpu.make_async_remote_copy(
                src_ref=weights.at[d, own_half],
                dst_ref=weights.at[d, own_half],
                send_sem=relay_send.at[d - 1],
                recv_sem=relay_recv.at[d - 1],
                device_id=(partner, my_col),
                device_id_type=mesh_id,
            )
        )
    for copy in weight_copies:
        copy.start()
    own_weight = pltpu.make_async_copy(w_out_ref, weights.at[0], weight_sem)
    own_weight.start()

    def project(role, w_ref):
        result = jnp.dot(tokens_ref[...], w_ref[...], preferred_element_type=jnp.float32).T
        for q in range(block_q):
            proj_ref[:, role, q * chans : (q + 1) * chans] = (
                result[:, q * LANES : (q + 1) * LANES]
                .reshape(rows, chans, LANES)
                .astype(jnp.bfloat16)
            )

    value_copies = row_copies(pl.ds(0, 1), value_send, value_recv)
    rest_copies = row_copies(pl.ds(1, 3), rest_send, rest_recv)
    own = pltpu.make_async_copy(proj_ref.at[my_row], recv.at[my_row], own_sem)
    project(0, w_value_ref)
    for copy in value_copies:
        copy.start()
    project(1, w_first_ref)
    project(2, w_second_ref)
    project(3, w_gate_ref)
    for copy in rest_copies:
        copy.start()
    own.start()
    twist_ref[...] = jnp.broadcast_to(
        small_twist_ref[...], (2, small_twist_ref.shape[1], chans, LANES)
    ).reshape(twist_ref.shape)

    features = features_ref[...]
    hidden = jnp.sin(
        jnp.dot(embed_ref[...], features, precision=precise, preferred_element_type=jnp.float32)
    )
    taps = jnp.dot(own_proj_ref[...], hidden.astype(jnp.bfloat16), preferred_element_type=jnp.float32)
    taps = taps * jnp.exp(-decay_ref[...] * features[0:1, :])
    line = lax.broadcasted_iota(jnp.int32, taps.shape, 0)
    lag = lax.broadcasted_iota(jnp.int32, taps.shape, 1)
    backward = ((line >= chans) & (line < 2 * chans)) | (line >= 3 * chans)
    taps_ref[...] = jnp.where(backward & (lag == 0), 0.0, taps).astype(jnp.bfloat16)

    half = first_ref.shape[0] // 2
    twist_cos, twist_sin = twist_ref.at[0], twist_ref.at[1]

    def ahead(signal):
        mid = jnp.dot(first_ref[...], signal, preferred_element_type=jnp.float32)
        real, imag = mid[:half], mid[half:]
        turned = jnp.concatenate(
            [
                real * twist_cos[...] + imag * twist_sin[...],
                imag * twist_cos[...] - real * twist_sin[...],
            ],
            axis=1,
        ).astype(jnp.bfloat16)
        return jnp.dot(turned, ahead_ref[...], preferred_element_type=jnp.float32)

    def convolve(signal, order):
        spec = ahead(signal.astype(jnp.bfloat16))
        real, imag = spec[:, :LANES], spec[:, LANES:]
        filt_real, filt_imag = spectra[order, 0], spectra[order, 1]
        prod = jnp.concatenate(
            [real * filt_real - imag * filt_imag, real * filt_imag + imag * filt_real], axis=1
        ).astype(jnp.bfloat16)
        mid = jnp.dot(prod, back_ref[...], preferred_element_type=jnp.float32)
        real, imag = mid[:, :LANES], mid[:, LANES:]
        turned = jnp.concatenate(
            [
                real * twist_cos[...] - imag * twist_sin[...],
                real * twist_sin[...] + imag * twist_cos[...],
            ],
            axis=0,
        ).astype(jnp.bfloat16)
        result = jnp.dot(last_ref[...], turned, preferred_element_type=jnp.float32)
        return result + gains_ref[:, 9 + order : 10 + order] * signal

    for order in range(2):
        for direction in range(2):
            base = (2 * order + direction) * chans
            signal = jnp.concatenate(
                [
                    taps_ref[base : base + chans, q * LANES : (q + 1) * LANES]
                    for q in range(length_q)
                ],
                axis=0,
            )
            spec = ahead(signal)
            if direction == 0:
                spectra[order, 0] = spec[:, :LANES]
                spectra[order, 1] = spec[:, LANES:]
            else:
                spectra[order, 0] += spec[:, :LANES]
                spectra[order, 1] -= spec[:, LANES:]

    def role_of(role):
        return recv[:, role].reshape(length_q * chans, LANES).astype(jnp.float32)

    def short(role):
        here = role_of(role)
        size = here.shape[0]
        lane = lax.broadcasted_iota(jnp.int32, here.shape, 1)
        blank = jnp.zeros((chans, LANES), jnp.float32)
        before = pltpu.roll(here, 1, 1)
        before = jnp.where(
            lane == 0, jnp.concatenate([blank, before[: size - chans]], axis=0), before
        )
        after = pltpu.roll(here, LANES - 1, 1)
        after = jnp.where(
            lane == LANES - 1, jnp.concatenate([after[chans:], blank], axis=0), after
        )
        w = lambda j: gains_ref[:, 3 * j + role : 3 * j + role + 1]
        return before * w(0) + here * w(1) + after * w(2)

    own.wait()
    for copy in value_copies:
        copy.wait_recv()
    conv = convolve(short(0), 0)
    for d in range(1, min(3, cols)):
        weight_copies[d - 1].wait_recv()
        relays[d - 1].start()
    for copy in rest_copies:
        copy.wait_recv()
    conv = convolve(short(1) * conv, 1)
    gate = role_of(3)
    outer = short(2) * conv * (gate / (1.0 + jnp.exp(-gate)))
    sent[...] = outer.astype(jnp.bfloat16).reshape(rows, block_q, chans, LANES)

    back_copies = []
    for d in range(1, rows):
        peer = lax.rem(my_row + d, rows)
        back_copies.append(
            pltpu.make_async_remote_copy(
                src_ref=sent.at[peer],
                dst_ref=recv_rows.at[my_row],
                send_sem=rows_send.at[d - 1],
                recv_sem=rows_recv.at[d - 1],
                device_id=(peer, my_col),
                device_id_type=mesh_id,
            )
        )
    for copy in back_copies:
        copy.start()
    for d in range(3, cols):
        weight_copies[d - 1].wait_recv()
        relays[d - 1].start()
    own = pltpu.make_async_copy(sent.at[my_row], recv_rows.at[my_row], own_sem)
    own.start()
    own.wait()
    for copy in back_copies:
        copy.wait_recv()

    col_copies = []
    for d in range(1, cols):
        peer = col_peer(d)
        col_copies.append(
            pltpu.make_async_remote_copy(
                src_ref=recv_rows.at[:, (peer * width) // LANES],
                dst_ref=recv_cols.at[d - 1],
                send_sem=cols_send.at[d - 1],
                recv_sem=cols_recv.at[d - 1],
                device_id=(my_row, peer),
                device_id_type=mesh_id,
            )
        )
    for copy in col_copies:
        copy.start()

    def turn(d, block):
        wide = block.reshape(rows * chans, LANES).astype(jnp.float32).T
        turned_rows[:, d * rows * chans : (d + 1) * rows * chans] = wide

    turn(0, recv_rows[:, (my_col * width) // LANES])
    own_weight.wait()
    for copy in col_copies:
        copy.wait_recv()
    for d in range(1, cols):
        turn(d, recv_cols[d - 1])
    for copy in relays:
        copy.wait_recv()
    shift = pl.multiple_of(lax.rem(my_col * width, LANES), width)
    picked = turned_rows[pl.ds(shift, width), :].astype(jnp.bfloat16)
    full = weights[...].reshape(cols * weights.shape[1], weights.shape[2])
    out_ref[...] = jnp.dot(picked, full, preferred_element_type=jnp.float32).astype(jnp.bfloat16)
    for copy in value_copies + rest_copies + back_copies + col_copies + weight_copies + relays:
        copy.wait_send()


def fast_body(
    tokens, w_value, w_first, w_second, w_gate, conv_taps, filter_embed, filter_freq, filter_proj,
    filter_decay, skip_gain, w_out,
):
    rows, cols = lax.axis_size("row"), lax.axis_size("col")
    tok_rows = tokens.shape[1]
    chan_col = w_value.shape[1]
    chans = chan_col // rows
    length = tok_rows * rows
    row_index = lax.axis_index("row")
    block_q = tok_rows // LANES
    length_q = length // LANES
    width = tok_rows // cols

    flat = tokens.reshape(tok_rows, tokens.shape[2])
    bands = (filter_embed.shape[0] - 1) // 2
    index = np.arange(length)
    spot = (index.astype(np.float32) / np.float32(length - 1)).astype(np.float32)
    phase = 2.0 * np.pi * (np.outer(np.arange(1, bands + 1), index) % length) / length
    features = np.concatenate([spot[None, :], np.cos(phase), np.sin(phase)]).astype(np.float32)
    embed = (filter_embed * filter_freq[None, :]).T
    own_proj = lax.dynamic_slice_in_dim(filter_proj, row_index * chans, chans, 3)
    own_proj = own_proj.reshape(own_proj.shape[0], 4 * chans).astype(jnp.bfloat16).T
    own_decay = lax.dynamic_slice_in_dim(filter_decay, row_index * chans, chans, 2).reshape(4 * chans, 1)

    own_taps = lax.dynamic_slice_in_dim(conv_taps, row_index * chans, chans, 2).reshape(9, chans)
    own_gain = lax.dynamic_slice_in_dim(skip_gain, row_index * chans, chans, 1)
    gains = jnp.tile(jnp.concatenate([own_taps, own_gain], axis=0).T, (length_q, 1))

    tables_in = dft_tables(length, chans)
    half = tables_in[0].shape[0] // 2
    vmem = pl.BlockSpec(memory_space=pltpu.VMEM)
    dma = pltpu.SemaphoreType.DMA
    mixed = pl.pallas_call(
        functools.partial(mixer_kernel, rows, cols, chans, width),
        out_shape=jax.ShapeDtypeStruct((width, w_out.shape[1]), jnp.bfloat16),
        in_specs=[vmem] * 5 + [pl.BlockSpec(memory_space=pl.ANY)] + [vmem] * 10,
        out_specs=vmem,
        scratch_shapes=[
            pltpu.VMEM((rows, 4, block_q * chans, LANES), jnp.bfloat16),
            pltpu.VMEM((rows, 4, block_q * chans, LANES), jnp.bfloat16),
            pltpu.VMEM((rows, block_q, chans, LANES), jnp.bfloat16),
            pltpu.VMEM((rows, block_q, chans, LANES), jnp.bfloat16),
            pltpu.VMEM((cols - 1, rows, chans, LANES), jnp.bfloat16),
            pltpu.VMEM((2, 2, half, LANES), jnp.float32),
            pltpu.VMEM((2, half, LANES), jnp.float32),
            pltpu.VMEM((cols, chan_col, w_out.shape[1]), jnp.bfloat16),
            pltpu.VMEM((LANES, cols * chan_col), jnp.float32),
            pltpu.VMEM((4 * chans, length), jnp.bfloat16),
            dma((rows - 1,)),
            dma((rows - 1,)),
            dma((rows - 1,)),
            dma((rows - 1,)),
            dma((rows - 1,)),
            dma((rows - 1,)),
            dma((cols - 1,)),
            dma((cols - 1,)),
            dma,
            dma((cols - 1,)),
            dma((cols - 1,)),
            dma((cols - 1,)),
            dma((cols - 1,)),
            dma,
        ],
        compiler_params=pltpu.CompilerParams(
            collective_id=0, has_side_effects=True, vmem_limit_bytes=48 * 1024 * 1024
        ),
        cost_estimate=pl.CostEstimate(flops=12_000_000_000, bytes_accessed=8_000_000, transcendentals=0),
    )(flat, w_value, w_first, w_second, w_gate, w_out, jnp.asarray(features), embed, own_proj, own_decay, gains, *tables_in)
    return mixed[None]


def shaped_body(tokens, w_value, *rest):
    rows, cols = lax.axis_size("row"), lax.axis_size("col")
    seqs, tok_rows = tokens.shape[:2]
    chan_col = w_value.shape[1]
    chans = chan_col // rows
    width = tok_rows // cols
    fits = (
        seqs == 1
        and rows % 2 == 0
        and chans % 32 == 0
        and tok_rows % LANES == 0
        and LANES % width == 0
        and tok_rows * chans <= 16384
    )
    return (fast_body if fits else body)(tokens, w_value, *rest)


def solution(mesh):
    in_specs = (
        P(None, "row", None),
        P(None, "col"),
        P(None, "col"),
        P(None, "col"),
        P(None, "col"),
        P(None, None, "col"),
        P(),
        P(),
        P(None, None, None, "col"),
        P(None, None, "col"),
        P(None, "col"),
        P("col", None),
    )
    out_specs = P(None, ("row", "col"), None)
    return jax.shard_map(shaped_body, mesh=mesh, in_specs=in_specs, out_specs=out_specs, check_vma=False)
```

profile of v0, /device:TPU:0, one launch (start us, length us, event | category | flops | bytes accessed | tf_op | source)
XLA Modules:
  0.0 52.0 jit_solution(8780638554968057099)
XLA Ops:
  0.0 0.0 copy-start
  0.0 0.8 %constant_dynamic-slice_fusion = f32[2,32]{1,0:T(2,128)S(1)} fusion(f32[2,256]{1,0:T(2,128)} %param.28, s32[]{:T(128)S(6)} %select_n.2), kind=kLoop, calls=%fused_computation.2 | loop fusion | bytes 516 | tf_op jit(solution)/shard_map/dynamic_slice | solution.py:514
  0.8 0.8 %constant_dynamic-slice_fusion.2 = f32[2,2,32]{2,1,0:T(2,128)S(1)} fusion(f32[2,2,256]{2,1,0:T(2,128)} %param.27, s32[]{:T(128)S(6)} %select_n.2), kind=kLoop, calls=%fused_computation.4 | loop fusion | bytes 1028 | tf_op jit(solution)/shard_map/dynamic_slice | solution.py:511
  1.6 0.8 %constant_dynamic-slice_fusion.1 = f32[3,3,32]{2,1,0:T(4,128)S(1)} fusion(f32[3,3,256]{2,1,0:T(4,128)} %param.23, s32[]{:T(128)S(6)} %select_n.2), kind=kLoop, calls=%fused_computation.3 | loop fusion | bytes 2308 | tf_op jit(solution)/shard_map/dynamic_slice | solution.py:513
  2.3 0.1 copy.30
  2.4 0.8 %copy.27 = f32[33,64]{0,1:T(8,128)S(1)} copy(f32[33,64]{1,0:T(8,128)} %param.24) | data formatting | bytes 16896 | tf_op args[6]
  3.2 0.7 %multiply_bitcast_fusion.embed_ref = f32[64,33]{1,0:T(8,128)S(1)} fusion(f32[33,64]{0,1:T(8,128)S(1)} %copy.27, f32[64]{0:T(128)} %param.25), kind=kLoop, calls=%fused_computation | loop fusion | flops 2112 | bytes 17152 | tf_op jit(solution)/shard_map/transpose | solution.py:508
  4.0 0.1 reshape.19.decay_ref
  4.1 0.0 copy-done
  4.1 0.1 constant_dynamic-slice_fusion.3
  4.2 0.1 copy.32
  4.4 0.0 copy-start.1
  4.4 1.2 %copy-done.1 = bf16[1,256,2048]{2,1,0:T(8,128)(2,1)S(1)} copy-done((bf16[1,256,2048]{2,1,0:T(8,128)(2,1)S(1)}, bf16[1,256,2048]{2,1,0:T(8,128)(2,1)}, u32[]{:S(2)}) %copy-start.1) | copy-done | bytes 1048600
  5.6 0.0 copy-start.2
  5.6 1.2 %copy-done.2 = bf16[2048,256]{1,0:T(8,128)(2,1)S(1)} copy-done((bf16[2048,256]{1,0:T(8,128)(2,1)S(1)}, bf16[2048,256]{1,0:T(8,128)(2,1)}, u32[]{:S(2)}) %copy-start.2) | copy-done | bytes 1048600
  6.8 0.0 copy-start.3
  6.8 1.2 %copy-done.3 = bf16[2048,256]{1,0:T(8,128)(2,1)S(1)} copy-done((bf16[2048,256]{1,0:T(8,128)(2,1)S(1)}, bf16[2048,256]{1,0:T(8,128)(2,1)}, u32[]{:S(2)}) %copy-start.3) | copy-done | bytes 1048600
  8.0 0.0 copy-start.4
  8.0 1.2 %copy-done.4 = bf16[2048,256]{1,0:T(8,128)(2,1)S(1)} copy-done((bf16[2048,256]{1,0:T(8,128)(2,1)S(1)}, bf16[2048,256]{1,0:T(8,128)(2,1)}, u32[]{:S(2)}) %copy-start.4) | copy-done | bytes 1048600
  9.3 0.0 copy-start.5
  9.3 1.0 %copy-done.5 = f32[33,2048]{1,0:T(8,128)S(1)} copy-done((f32[33,2048]{1,0:T(8,128)S(1)}, f32[33,2048]{1,0:T(8,128)}, u32[]{:S(2)}) %copy-start.5) | copy-done | bytes 270360
  10.2 0.0 copy-start.6
  10.2 0.9 %copy-done.6 = bf16[256,256]{1,0:T(8,128)(2,1)S(1)} copy-done((bf16[256,256]{1,0:T(8,128)(2,1)S(1)}, bf16[256,256]{1,0:T(8,128)(2,1)}, u32[]{:S(2)}) %copy-start.6) | copy-done | bytes 131096
  11.2 0.0 copy-start.7
  11.2 0.9 %copy-done.7 = bf16[256,256]{1,0:T(8,128)(2,1)S(1)} copy-done((bf16[256,256]{1,0:T(8,128)(2,1)S(1)}, bf16[256,256]{1,0:T(8,128)(2,1)}, u32[]{:S(2)}) %copy-start.7) | copy-done | bytes 131096
  12.1 0.0 copy-start.8
  12.1 0.7 %copy-done.8 = f32[2,17,1,128]{3,2,1,0:T(1,128)S(1)} copy-done((f32[2,17,1,128]{3,2,1,0:T(1,128)S(1)}, f32[2,17,1,128]{3,2,1,0:T(1,128)}, u32[]{:S(2)}) %copy-start.8) | copy-done | bytes 17432
  12.8 38.5 %shard_map.172 = bf16[64,2048]{1,0:T(8,128)(2,1)S(1)} custom-call(bf16[256,2048]{1,0:T(8,128)(2,1)S(1)} %bitcast.13, bf16[2048,256]{1,0:T(8,128)(2,1)S(1)} %copy-done.2, bf16[2048,256]{1,0:T(8,128)(2,1)S(1)} %copy-done.3, bf16[2048,256]{1,0:T(8,128)(2,1)S(1)} %copy-done.4, bf16[2048,256]{1,0:T(8,128)(2,1)} %w_gate_ref.1, bf16[256,2048]{1,0:T(8,128)(2,1)} %w_out_ref.1, ...), custom_call_target="tpu_custom_call" | custom-call | flops 12000000000 | bytes 8000000 | tf_op jit(solution)/shard_map/pallas_call | solution.py:521
  51.3 0.7 %copy.34 = bf16[1,64,2048]{2,1,0:T(8,128)(2,1)} copy(bf16[1,64,2048]{2,1,0:T(8,128)(2,1)S(1)} %bitcast.11) | data formatting | bytes 524288
  (3 shorter events, 0.0 us)
Async XLA Ops:
  0.0 4.1 %copy-start = (f32[64,2,2,256]{3,2,1,0:T(2,128)S(1)}, f32[64,2,2,256]{3,2,1,0:T(2,128)}, u32[]{:S(2)}) copy-start(f32[64,2,2,256]{3,2,1,0:T(2,128)} %param.26) | copy-start | bytes 786436
  4.4 1.2 %copy-start.1 = (bf16[1,256,2048]{2,1,0:T(8,128)(2,1)S(1)}, bf16[1,256,2048]{2,1,0:T(8,128)(2,1)}, u32[]{:S(2)}) copy-start(bf16[1,256,2048]{2,1,0:T(8,128)(2,1)} %param.18) | copy-start | bytes 3145732
  5.6 1.2 %copy-start.2 = (bf16[2048,256]{1,0:T(8,128)(2,1)S(1)}, bf16[2048,256]{1,0:T(8,128)(2,1)}, u32[]{:S(2)}) copy-start(bf16[2048,256]{1,0:T(8,128)(2,1)} %w_value_ref.1) | copy-start | bytes 3145732
  6.8 1.2 %copy-start.3 = (bf16[2048,256]{1,0:T(8,128)(2,1)S(1)}, bf16[2048,256]{1,0:T(8,128)(2,1)}, u32[]{:S(2)}) copy-start(bf16[2048,256]{1,0:T(8,128)(2,1)} %w_first_ref.1) | copy-start | bytes 3145732
  8.0 1.2 %copy-start.4 = (bf16[2048,256]{1,0:T(8,128)(2,1)S(1)}, bf16[2048,256]{1,0:T(8,128)(2,1)}, u32[]{:S(2)}) copy-start(bf16[2048,256]{1,0:T(8,128)(2,1)} %w_second_ref.1) | copy-start | bytes 3145732
  9.3 1.0 %copy-start.5 = (f32[33,2048]{1,0:T(8,128)S(1)}, f32[33,2048]{1,0:T(8,128)}, u32[]{:S(2)}) copy-start(f32[33,2048]{1,0:T(8,128)} %constant.29.clone.features_ref) | copy-start | bytes 811012
  10.2 0.9 %copy-start.6 = (bf16[256,256]{1,0:T(8,128)(2,1)S(1)}, bf16[256,256]{1,0:T(8,128)(2,1)}, u32[]{:S(2)}) copy-start(bf16[256,256]{1,0:T(8,128)(2,1)} %constant.33.back_ref) | copy-start | bytes 393220
  11.2 0.9 %copy-start.7 = (bf16[256,256]{1,0:T(8,128)(2,1)S(1)}, bf16[256,256]{1,0:T(8,128)(2,1)}, u32[]{:S(2)}) copy-start(bf16[256,256]{1,0:T(8,128)(2,1)} %constant.32.ahead_ref) | copy-start | bytes 393220
  12.1 0.7 %copy-start.8 = (f32[2,17,1,128]{3,2,1,0:T(1,128)S(1)}, f32[2,17,1,128]{3,2,1,0:T(1,128)}, u32[]{:S(2)}) copy-start(f32[2,17,1,128]{3,2,1,0:T(1,128)} %constant.26.clone.small_twist_ref) | copy-start | bytes 52228
where the time goes:
time: 52.6 us; the launch traced here: 52 us
  Pallas kernels  38.5 us (73%)
  local copies, waits for them, and re-layouts  12.7 us (24%)
  other arithmetic  0.74 us (1%)
    pallas_call x1, Pallas kernels, fast_body(): pl.pallas_call(functools.partial(mixer_kernel, rows, cols, chans, width),...  38.5 us
    unnamed x21, local copies, waits for them, and re-layouts  10 us

commit v1 on v0

v1 whole, which is shorter than its diff:
```python
import functools
import math

import jax
import jax.numpy as jnp
import numpy as np
from jax import lax
from jax.experimental import pallas as pl
from jax.experimental.pallas import tpu as pltpu
from jax.sharding import PartitionSpec as P

precise = lax.Precision.HIGHEST


def padded_2(array, sides, width):
    for axis, dim in sides:
        size, length = (lax.axis_size(axis), array.shape[dim])
        up = [(i, (i + 1) % size) for i in range(size - 1)]
        down = [(j, i) for i, j in up]
        last = lax.slice_in_dim(array, length - width, length, axis=dim)
        leading = lax.slice_in_dim(array, 0, width, axis=dim)
        before = lax.ppermute(last, axis, up)
        after = lax.ppermute(leading, axis, down)
        array = jnp.concatenate([before, array, after], axis=dim)
    return array


def split_length(total):
    factor = math.isqrt(total)
    while total % factor != 0:
        factor = factor - 1
    return (factor, total // factor)


def tables(outer, inner, total):
    first_index = jnp.arange(outer, dtype=jnp.int32)
    second_index = jnp.arange(inner, dtype=jnp.int32)
    scale = 2.0 * math.pi
    outer_angle = (first_index[:, None] * first_index[None, :] % outer).astype(jnp.float32) * (
        scale / outer
    )
    inner_angle = (second_index[:, None] * second_index[None, :] % inner).astype(jnp.float32) * (
        scale / inner
    )
    twist_angle = (first_index[:, None] * second_index[None, :] % total).astype(jnp.float32) * (
        scale / total
    )
    return (
        jnp.cos(outer_angle),
        jnp.sin(outer_angle),
        jnp.cos(inner_angle),
        jnp.sin(inner_angle),
        jnp.cos(twist_angle),
        jnp.sin(twist_angle),
    )


def forward_real(signal, table):
    outer_cos, outer_sin, inner_cos, inner_sin, twist_cos, twist_sin = table
    outer = outer_cos.shape[0]
    inner = inner_cos.shape[0]
    grid = signal.reshape(signal.shape[0], outer, inner)
    real_part = jnp.einsum("kq,cqp->ckp", outer_cos, grid, precision=precise)
    imag_part = -jnp.einsum("kq,cqp->ckp", outer_sin, grid, precision=precise)
    turned_real = real_part * twist_cos + imag_part * twist_sin
    turned_imag = imag_part * twist_cos - real_part * twist_sin
    spec_real = jnp.einsum("ckp,pj->ckj", turned_real, inner_cos, precision=precise) + jnp.einsum(
        "ckp,pj->ckj", turned_imag, inner_sin, precision=precise
    )
    spec_imag = jnp.einsum("ckp,pj->ckj", turned_imag, inner_cos, precision=precise) - jnp.einsum(
        "ckp,pj->ckj", turned_real, inner_sin, precision=precise
    )
    return (spec_real, spec_imag)


def inverse_real(spec_real, spec_imag, table):
    outer_cos, outer_sin, inner_cos, inner_sin, twist_cos, twist_sin = table
    total = outer_cos.shape[0] * inner_cos.shape[0]
    back_real = jnp.einsum("ckj,jp->ckp", spec_real, inner_cos, precision=precise) - jnp.einsum(
        "ckj,jp->ckp", spec_imag, inner_sin, precision=precise
    )
    back_imag = jnp.einsum("ckj,jp->ckp", spec_real, inner_sin, precision=precise) + jnp.einsum(
        "ckj,jp->ckp", spec_imag, inner_cos, precision=precise
    )
    turned_real = back_real * twist_cos - back_imag * twist_sin
    turned_imag = back_real * twist_sin + back_imag * twist_cos
    result = jnp.einsum("qk,ckp->cqp", outer_cos, turned_real, precision=precise) - jnp.einsum(
        "qk,ckp->cqp", outer_sin, turned_imag, precision=precise
    )
    return result.reshape(result.shape[0], total) / total


def channel_filters(
    length, row_index, chan_row, filter_embed, filter_freq, filter_proj, filter_decay
):
    bands = (filter_embed.shape[0] - 1) // 2
    index = jnp.arange(length, dtype=jnp.int32)
    spot = index.astype(jnp.float32) / (length - 1)
    freqs = jnp.arange(1, bands + 1, dtype=jnp.int32)
    phase = (index[:, None] * freqs[None, :] % length).astype(jnp.float32) * (
        2.0 * math.pi / length
    )
    features = jnp.concatenate([spot[:, None], jnp.cos(phase), jnp.sin(phase)], axis=1)
    hidden = jnp.sin(filter_freq[None, :] * jnp.dot(features, filter_embed, precision=precise))
    own_proj = lax.dynamic_slice_in_dim(filter_proj, row_index * chan_row, chan_row, 3)
    own_decay = lax.dynamic_slice_in_dim(filter_decay, row_index * chan_row, chan_row, 2)
    taps = jnp.dot(hidden, own_proj.reshape(own_proj.shape[0], 4 * chan_row), precision=precise)
    taps = jnp.transpose(taps).reshape(2, 2, chan_row, length)
    taps = taps * jnp.exp(-spot[None, None, None, :] * own_decay[:, :, :, None])
    cycles = []
    for order in range(2):
        behind = jnp.flip(taps[order, 1, :, 1:], axis=1)
        cycles.append(
            jnp.concatenate([taps[order, 0], jnp.zeros((chan_row, 1), jnp.float32), behind], axis=1)
        )
    return cycles


def body(
    tokens,
    w_value,
    w_first,
    w_second,
    w_gate,
    conv_taps,
    filter_embed,
    filter_freq,
    filter_proj,
    filter_decay,
    skip_gain,
    w_out,
):
    seq_count = tokens.shape[0]
    tok_rows = tokens.shape[1]
    chan_col = w_value.shape[1]
    row_count = lax.axis_size("row")
    chan_row = chan_col // row_count
    length = tok_rows * row_count
    row_index = lax.axis_index("row")
    proj = jnp.concatenate(
        [
            jnp.dot(tokens, w_value, preferred_element_type=jnp.float32),
            jnp.dot(tokens, w_first, preferred_element_type=jnp.float32),
            jnp.dot(tokens, w_second, preferred_element_type=jnp.float32),
        ],
        axis=2,
    ).astype(jnp.bfloat16)
    gate = jnp.dot(tokens, w_gate, preferred_element_type=jnp.float32).astype(jnp.bfloat16)
    padded = padded_2(proj, (("row", 1),), 1).astype(jnp.float32)
    weights = conv_taps.reshape(3, 3 * chan_col)
    short = padded[:, :-2] * weights[0] + padded[:, 1:-1] * weights[1] + padded[:, 2:] * weights[2]
    value_rows = jnp.transpose(short[:, :, :chan_col], (0, 2, 1))
    first_rows = jnp.transpose(short[:, :, chan_col : 2 * chan_col], (0, 2, 1))
    second_rows = jnp.transpose(short[:, :, 2 * chan_col :], (0, 2, 1))
    outer, inner = split_length(2 * length)
    table = tables(outer, inner, 2 * length)
    cycles = channel_filters(
        length, row_index, chan_row, filter_embed, filter_freq, filter_proj, filter_decay
    )
    spectra = [forward_real(cycle, table) for cycle in cycles]
    own_gain = lax.dynamic_slice_in_dim(skip_gain, row_index * chan_row, chan_row, 1)

    def convolve(signal, order):
        flat = signal.reshape(seq_count * chan_row, length)
        padded_signal = jnp.concatenate([flat, jnp.zeros_like(flat)], axis=1)
        sig_real, sig_imag = forward_real(padded_signal, table)
        sig_real = sig_real.reshape(seq_count, chan_row, outer, inner)
        sig_imag = sig_imag.reshape(seq_count, chan_row, outer, inner)
        filt_real, filt_imag = spectra[order]
        prod_real = sig_real * filt_real[None] - sig_imag * filt_imag[None]
        prod_imag = sig_real * filt_imag[None] + sig_imag * filt_real[None]
        result = inverse_real(
            prod_real.reshape(seq_count * chan_row, outer, inner),
            prod_imag.reshape(seq_count * chan_row, outer, inner),
            table,
        )[:, :length]
        return result.reshape(seq_count, chan_row, length) + own_gain[order][None, :, None] * signal

    value_chan, first_chan = (
        lax.all_to_all(value_rows, "row", split_axis=1, concat_axis=2, tiled=True),
        lax.all_to_all(first_rows, "row", split_axis=1, concat_axis=2, tiled=True),
    )
    inner_chan = first_chan * convolve(value_chan, 0)
    second_conv = lax.all_to_all(
        convolve(inner_chan, 1), "row", split_axis=2, concat_axis=1, tiled=True
    )
    outer_rows = (
        jnp.transpose(second_rows * second_conv, (0, 2, 1)) * jax.nn.silu(gate.astype(jnp.float32))
    ).astype(jnp.bfloat16)
    own_rows = tok_rows // lax.axis_size("col")
    flat_rows = jnp.transpose(outer_rows, (1, 0, 2)).reshape(tok_rows * seq_count, chan_col)
    summed = lax.psum_scatter(
        jnp.dot(flat_rows, w_out, preferred_element_type=jnp.float32).astype(jnp.bfloat16),
        "col",
        scatter_dimension=0,
        tiled=True,
    ).astype(jnp.float32)
    summed = jnp.transpose(summed.reshape(own_rows, seq_count, w_out.shape[1]), (1, 0, 2))
    return summed.astype(jnp.bfloat16)


LANES = 128
PACK = 16


def dft_tables(length):
    filled = length // LANES
    outer = 2 * filled
    total = outer * LANES
    half = filled + 1
    eye = np.eye(PACK)
    q, k, p = np.arange(filled), np.arange(half), np.arange(LANES)
    inside = k[1:-1]
    angle = 2.0 * np.pi * (np.outer(k, q) % outer) / outer
    first = np.concatenate([np.kron(np.cos(angle), eye), np.kron(-np.sin(angle)[inside], eye)], axis=0)
    weight = np.where((k == 0) | (k == filled), 1.0, 2.0) / total
    last = np.concatenate(
        [
            np.kron(np.cos(angle).T * weight, eye),
            np.kron((-np.sin(angle).T * weight)[:, inside], eye),
        ],
        axis=1,
    )
    turn = 2.0 * np.pi * np.outer(k, p) / total
    twist = np.stack([np.cos(turn), np.sin(turn)])[:, :, None, :]
    twist = np.broadcast_to(twist, (2, half, 8, LANES))
    angle = 2.0 * np.pi * (np.outer(p, p) % LANES) / LANES
    cos, sin = np.cos(angle), np.sin(angle)
    ahead = np.block([[cos, -sin], [sin, cos]])
    back = np.block([[cos, sin], [-sin, cos]])
    low = lambda array: jnp.asarray(array.astype(np.float32)).astype(jnp.bfloat16)
    return low(first), low(last), jnp.asarray(twist.astype(np.float32)), low(ahead), low(back)


def split_bf16(array):
    high = array.astype(jnp.bfloat16).astype(jnp.float32)
    middle = (array - high).astype(jnp.bfloat16).astype(jnp.float32)
    low = (array - high - middle).astype(jnp.bfloat16).astype(jnp.float32)
    return high, middle, low


def host_split(array):
    low_type = jnp.bfloat16.dtype
    high = array.astype(low_type).astype(np.float64)
    middle = (array - high).astype(low_type).astype(np.float64)
    low = (array - high - middle).astype(low_type).astype(np.float64)
    return high, middle, low


def flip(value, bits):
    bit = 1
    while bit <= bits:
        if bits & bit:
            value = value + bit - 2 * bit * lax.rem(lax.div(value, bit), 2)
        bit *= 2
    return value


def mixer_kernel(
    rows, cols, width, emb,
    tokens_hbm, w_value_hbm, w_first_hbm, w_second_hbm, w_gate_hbm, w_out_hbm, conv_hbm, embed_hbm, freq_hbm,
    proj_hbm, decay_hbm, gain_hbm, features_hbm, first_hbm, last_hbm, twist_hbm, ahead_hbm, back_hbm, perm_hbm,
    out_ref,
    tokens_ref, w_refs, conv_ref, embed_ref, freq_ref, fproj_ref, decay_ref, gain_ref, features_ref, first_ref,
    last_ref, twist_ref, ahead_ref, back_ref, perm_ref,
    send, recv, spectra, taps_ref, stack_ref, coef_ref, gated, gated_in, edge_out, edge_in, piece, final, weights,
    load_sem, row_send, row_recv, edge_send, edge_recv, gate_send, gate_recv, piece_send, piece_recv,
    wide_send, wide_recv, pass_send, pass_recv, mate_send, mate_recv,
):
    my_row = lax.axis_index("row")
    my_col = lax.axis_index("col")
    mesh_id = pl.DeviceIdType.MESH
    groups = recv.shape[2]
    chans = groups * PACK
    tok_rows = tokens_ref.shape[0]
    block_q = tok_rows // LANES
    length_q = rows * block_q
    length = tok_rows * rows
    half = length_q + 1
    hid = freq_ref.shape[1]
    f32, low = jnp.float32, jnp.bfloat16

    def remote(src, dst, send_sem, recv_sem, row, col):
        return pltpu.make_async_remote_copy(
            src_ref=src, dst_ref=dst, send_sem=send_sem, recv_sem=recv_sem,
            device_id=(row, col), device_id_type=mesh_id,
        )

    barrier = pltpu.get_barrier_semaphore()
    for d in range(1, rows):
        pl.semaphore_signal(barrier, inc=1, device_id=(flip(my_row, d), my_col), device_id_type=mesh_id)
    for d in range(1, cols):
        pl.semaphore_signal(barrier, inc=1, device_id=(my_row, flip(my_col, d)), device_id_type=mesh_id)

    loads = {}
    for name, src, dst in (
        ("tokens", tokens_hbm, tokens_ref),
        ("value", w_value_hbm, w_refs.at[0]),
        ("embed", embed_hbm, embed_ref.at[pl.ds(0, emb)]),
        ("freq", freq_hbm, freq_ref),
        ("conv", conv_hbm, conv_ref),
        ("gain", gain_hbm, gain_ref),
        ("decay", decay_hbm, decay_ref),
        ("first", w_first_hbm, w_refs.at[1]),
        ("second", w_second_hbm, w_refs.at[2]),
        ("gate", w_gate_hbm, w_refs.at[3]),
        ("fproj", proj_hbm, fproj_ref),
        ("features", features_hbm, features_ref),
        ("dft_first", first_hbm, first_ref),
        ("twist", twist_hbm, twist_ref),
        ("ahead", ahead_hbm, ahead_ref),
        ("perm", perm_hbm, perm_ref),
        ("back", back_hbm, back_ref),
        ("dft_last", last_hbm, last_ref),
        ("w_out", w_out_hbm, weights.at[0]),
    ):
        loads[name] = pltpu.make_async_copy(src, dst, load_sem.at[len(loads)])
        loads[name].start()

    side = lax.rem(my_row, 2)
    mate = flip(my_row, 1)
    quarter = rows // 4
    rows_of = lambda part: pl.ds(side * (rows // 2) + part * quarter, quarter)

    def wide_copy(index, d, part):
        return remote(
            w_out_hbm.at[rows_of(part)], weights.at[d, rows_of(part)],
            wide_send.at[index], wide_recv.at[index], my_row, flip(my_col, d),
        )

    wide = {(1, 0): wide_copy(0, 1, 0), (2, 1): wide_copy(1, 2, 1), (1, 1): wide_copy(2, 1, 1), (2, 0): wide_copy(3, 2, 0)}
    passed = {
        0: remote(weights.at[1, rows_of(0)], weights.at[3, rows_of(0)], pass_send.at[0], pass_recv.at[0], my_row, flip(my_col, 2)),
        1: remote(weights.at[2, rows_of(1)], weights.at[3, rows_of(1)], pass_send.at[1], pass_recv.at[1], my_row, flip(my_col, 1)),
    }
    mates = {}
    for d in range(1, cols):
        for part in range(2):
            index = 2 * (d - 1) + part
            mates[d, part] = remote(
                weights.at[d, rows_of(part)], weights.at[d, rows_of(part)],
                mate_send.at[index], mate_recv.at[index], mate, my_col,
            )

    far_first = sorted(range(1, rows), key=lambda d: -(d & (rows // 2)))

    def row_copies(role):
        return [
            remote(
                send.at[role, flip(my_row, d)], recv.at[role, my_row],
                row_send.at[role, d - 1], row_recv.at[role, d - 1], flip(my_row, d), my_col,
            )
            for d in far_first
        ]

    def project(role):
        return jnp.dot(tokens_ref[...], w_refs[role], preferred_element_type=f32)

    def project_turned(role):
        result = project(role).T
        for q in range(block_q):
            send[role, :, :, q] = (
                result[:, q * LANES : (q + 1) * LANES].reshape(rows, groups, PACK, LANES).astype(low)
            )

    value_copies, first_copies = row_copies(0), row_copies(1)

    loads["tokens"].wait()
    loads["value"].wait()
    project_turned(0)
    pl.semaphore_wait(barrier, rows + cols - 2)
    for copy in value_copies:
        copy.start()
    wide[1, 0].start()
    wide[2, 1].start()
    recv[0, my_row] = send[0, my_row]

    loads["first"].wait()
    project_turned(1)
    for copy in first_copies:
        copy.start()
    recv[1, my_row] = send[1, my_row]

    loads["second"].wait()
    second = project(2).astype(low).astype(f32)
    edge_out[0] = jnp.broadcast_to(second[tok_rows - 1 :], edge_out.shape[1:])
    edge_out[1] = jnp.broadcast_to(second[:1], edge_out.shape[1:])
    edges = [
        remote(edge_out.at[0], edge_in.at[0], edge_send.at[0], edge_recv.at[0], lax.rem(my_row + 1, rows), my_col),
        remote(edge_out.at[1], edge_in.at[1], edge_send.at[1], edge_recv.at[1], lax.rem(my_row + rows - 1, rows), my_col),
    ]
    for copy in edges:
        copy.start()
    loads["gate"].wait()
    gate = project(3).astype(low).astype(f32)
    loads["conv"].wait()

    loads["gain"].wait()
    loads["decay"].wait()
    stack_ref[...] = jnp.zeros_like(stack_ref)
    for j in range(3):
        stack_ref[j : j + 1] = conv_ref[j, 0:1]
        stack_ref[3 + j : 4 + j] = conv_ref[j, 1:2]
    stack_ref[6:8] = gain_ref[...]
    stack_ref[8:10] = decay_ref[0]
    stack_ref[10:12] = decay_ref[1]
    shape = (chans, stack_ref.shape[1])
    picks = lax.broadcasted_iota(jnp.int32, shape, 1) == lax.broadcasted_iota(jnp.int32, shape, 0) + my_row * chans
    picks = jnp.where(picks, 1.0, 0.0)
    contract_last = (((1,), (1,)), ((), ()))
    own = lax.dot_general(picks, stack_ref[...], contract_last, precision=precise, preferred_element_type=f32)
    for k in range(8):
        coef_ref[k] = jnp.broadcast_to(own[:, k : k + 1], (chans, LANES)).reshape(groups, PACK, LANES)

    loads["embed"].wait()
    loads["freq"].wait()
    embed = embed_ref[...] * (freq_ref[...] * (1.0 / math.pi))
    embed = jnp.where(lax.broadcasted_iota(jnp.int32, embed.shape, 0) < emb, embed, 0.0)
    high, middle, least = split_bf16(embed)
    stacked = jnp.concatenate([high, high, middle, high, middle, least], axis=0).astype(low)
    loads["features"].wait()
    turns = lax.dot_general(stacked, features_ref[...], (((0,), (0,)), ((), ())), preferred_element_type=f32)
    whole = jnp.floor(turns + 0.5)
    rest = turns - whole
    sign = 1.0 - 2.0 * (whole - 2.0 * jnp.floor(whole * 0.5))
    square = rest * rest
    series = jnp.full_like(square, -(math.pi**11) / math.factorial(11))
    for n in (9, 7, 5, 3, 1):
        series = series * square + (-1) ** (n // 2) * math.pi**n / math.factorial(n)
    hidden = (series * (rest * sign)).astype(low)
    loads["fproj"].wait()
    pieces = []
    picks_low = picks.astype(low)
    halves = 2
    for od in range(4):
        parts = [
            fproj_ref[pl.ds((od // 2) * 2 * halves + j * 2 + od % 2, hid, stride=4 * halves), :]
            for j in range(halves)
        ]
        block = jnp.concatenate(parts, axis=1).astype(low)
        pieces.append(lax.dot_general(picks_low, block, contract_last, preferred_element_type=f32).astype(low))
    taps = jnp.dot(jnp.concatenate(pieces, axis=0), hidden, preferred_element_type=f32)
    lag = lax.broadcasted_iota(jnp.int32, (1, length), 1)
    spot = lag.astype(f32) / (length - 1)
    for od in range(4):
        block = taps[od * chans : (od + 1) * chans] * jnp.exp(-own[:, 8 + od : 9 + od] * spot)
        if od % 2 == 1:
            block = jnp.where(lag == 0, 0.0, block)
        taps_ref[od] = block.astype(low)

    def wide_twist(index):
        return twist_ref[index].reshape(half, 1, 8, LANES)

    def ahead(signal):
        mid = jnp.dot(first_ref[...], signal, preferred_element_type=f32)
        blank = jnp.zeros((PACK, LANES), f32)
        blocks = []
        for g in range(groups):
            lanes = slice(g * LANES, (g + 1) * LANES)
            real = mid[: half * PACK, lanes].reshape(half, 2, 8, LANES)
            imag = jnp.concatenate([blank, mid[half * PACK :, lanes], blank], axis=0).reshape(half, 2, 8, LANES)
            cos, sin = wide_twist(0), wide_twist(1)
            blocks.append(
                jnp.concatenate(
                    [
                        (real * cos + imag * sin).reshape(half * PACK, LANES),
                        (imag * cos - real * sin).reshape(half * PACK, LANES),
                    ],
                    axis=1,
                ).astype(low)
            )
        return jnp.dot(jnp.concatenate(blocks, axis=0), ahead_ref[...], preferred_element_type=f32)

    def convolve(signal, order):
        spec = ahead(signal.astype(low))
        real, imag = spec[:, :LANES], spec[:, LANES:]
        filt_real, filt_imag = spectra[order, 0], spectra[order, 1]
        prod = jnp.concatenate(
            [real * filt_real - imag * filt_imag, real * filt_imag + imag * filt_real], axis=1
        ).astype(low)
        mid = jnp.dot(prod, back_ref[...], preferred_element_type=f32)
        blocks = []
        for g in range(groups):
            span = slice(g * half * PACK, (g + 1) * half * PACK)
            real = mid[span, :LANES].reshape(half, 2, 8, LANES)
            imag = mid[span, LANES:].reshape(half, 2, 8, LANES)
            cos, sin = wide_twist(0), wide_twist(1)
            turned_real = (real * cos - imag * sin).reshape(half * PACK, LANES)
            turned_imag = (real * sin + imag * cos)[1:-1].reshape((half - 2) * PACK, LANES)
            blocks.append(jnp.concatenate([turned_real, turned_imag], axis=0).astype(low))
        result = jnp.dot(last_ref[...], jnp.concatenate(blocks, axis=1), preferred_element_type=f32)
        gain = jnp.concatenate([coef_ref[6 + order, g] for g in range(groups)], axis=1)
        shape = (length_q, PACK, groups * LANES)
        return (result.reshape(shape) + gain[None] * signal.reshape(shape)).reshape(signal.shape)

    loads["dft_first"].wait()
    loads["twist"].wait()
    loads["ahead"].wait()
    for order in range(2):
        for direction in range(2):
            od = 2 * order + direction
            signal = jnp.concatenate(
                [
                    jnp.concatenate(
                        [
                            taps_ref[od, g * PACK : (g + 1) * PACK, q * LANES : (q + 1) * LANES]
                            for q in range(length_q)
                        ],
                        axis=0,
                    )
                    for g in range(groups)
                ],
                axis=1,
            )
            spec = ahead(signal)
            if direction == 0:
                spectra[order, 0] = spec[:, :LANES]
                spectra[order, 1] = spec[:, LANES:]
            else:
                spectra[order, 0] += spec[:, :LANES]
                spectra[order, 1] -= spec[:, LANES:]

    for copy in edges:
        copy.wait_recv()
    line = lax.broadcasted_iota(jnp.int32, second.shape, 0)
    above = jnp.where(my_row == 0, 0.0, edge_in[0, 0:1])
    below = jnp.where(my_row == rows - 1, 0.0, edge_in[1, 0:1])
    before = jnp.where(line == 0, above, pltpu.roll(second, 1, 0))
    after = jnp.where(line == tok_rows - 1, below, pltpu.roll(second, tok_rows - 1, 0))
    short_second = before * conv_ref[0, 2:3] + second * conv_ref[1, 2:3] + after * conv_ref[2, 2:3]
    both = (short_second * (gate / (1.0 + jnp.exp(-gate)))).astype(low)
    loads["perm"].wait()
    both = jnp.dot(both, perm_ref[...], preferred_element_type=f32).astype(low)
    per_group = rows * PACK
    for g in range(groups):
        gated[:, g] = both[:, g * per_group : (g + 1) * per_group].reshape(cols, width, per_group)
    gate_copies = [
        remote(
            gated.at[flip(my_col, d)], gated_in.at[d], gate_send.at[d - 1], gate_recv.at[d - 1], my_row, flip(my_col, d)
        )
        for d in range(1, cols)
    ]
    for copy in gate_copies:
        copy.start()
    gated_in[0] = gated[my_col]
    wide[1, 1].start()
    wide[2, 0].start()

    def short(role):
        blocks = []
        for g in range(groups):
            here = recv[role, :, g].reshape(length_q * PACK, LANES).astype(f32)
            size = here.shape[0]
            lane = lax.broadcasted_iota(jnp.int32, here.shape, 1)
            blank = jnp.zeros((PACK, LANES), f32)
            before = pltpu.roll(here, 1, 1)
            before = jnp.where(lane == 0, jnp.concatenate([blank, before[: size - PACK]], axis=0), before)
            after = pltpu.roll(here, LANES - 1, 1)
            after = jnp.where(lane == LANES - 1, jnp.concatenate([after[PACK:], blank], axis=0), after)
            shape = (length_q, PACK, LANES)
            w = lambda j: coef_ref[3 * role + j, g][None]
            result = before.reshape(shape) * w(0) + here.reshape(shape) * w(1) + after.reshape(shape) * w(2)
            blocks.append(result.reshape(size, LANES))
        return jnp.concatenate(blocks, axis=1)

    loads["back"].wait()
    loads["dft_last"].wait()
    for copy in value_copies:
        copy.wait_recv()
    conv = convolve(short(0), 0)
    for copy in first_copies:
        copy.wait_recv()
    conv = convolve(short(1) * conv, 1)

    left = conv[:, :LANES].reshape(length_q, PACK, LANES)
    right = conv[:, LANES:].reshape(length_q, PACK, LANES)
    lane = lax.broadcasted_iota(jnp.int32, left.shape, 2)
    piece[:, 0] = jnp.where(lane < width, left, pltpu.roll(right, width, 2)).astype(low)
    piece[:, 1] = jnp.where(lane < width, pltpu.roll(left, width, 2), right).astype(low)
    piece_copies = []
    for dr in far_first + [0]:
        for dc in range(cols):
            if dr == 0 and dc == 0:
                continue
            row, col = flip(my_row, dr), flip(my_col, dc)
            index = dr * cols + dc - 1
            piece_copies.append(
                remote(
                    piece.at[row * block_q + lax.div(col, 2), lax.rem(col, 2)], final.at[dc, my_row],
                    piece_send.at[index], piece_recv.at[index], row, col,
                )
            )
    for copy in piece_copies:
        copy.start()
    final[0, my_row] = piece[my_row * block_q + lax.div(my_col, 2), lax.rem(my_col, 2)]

    wide[1, 0].wait_recv()
    passed[0].start()
    mates[1, 0].start()
    wide[2, 1].wait_recv()
    passed[1].start()
    mates[2, 1].start()
    wide[1, 1].wait_recv()
    mates[1, 1].start()
    wide[2, 0].wait_recv()
    mates[2, 0].start()
    for part in range(2):
        passed[part].wait_recv()
        mates[3, part].start()

    for copy in gate_copies:
        copy.wait_recv()
    for copy in piece_copies:
        copy.wait_recv()
    loads["w_out"].wait()
    picked = []
    for d in range(cols):
        outer = final[d].reshape(rows * PACK, LANES).astype(f32).T
        outer = (outer * gated_in[d].reshape(groups * width, per_group).astype(f32)).astype(low)
        for g in range(groups):
            picked.append(outer[g * width : (g + 1) * width])
    for copy in mates.values():
        copy.wait_recv()
    depth = weights.shape[4]
    full = jnp.concatenate(
        [weights[d, :, g].reshape(per_group, depth) for d in range(cols) for g in range(groups)], axis=0
    )
    out_ref[...] = jnp.dot(jnp.concatenate(picked, axis=1), full, preferred_element_type=f32).astype(low)
    for copy in value_copies + first_copies + edges + gate_copies + piece_copies:
        copy.wait_send()
    for group in (wide, passed, mates):
        for copy in group.values():
            copy.wait_send()


def fast_body(
    tokens, w_value, w_first, w_second, w_gate, conv_taps, filter_embed, filter_freq, filter_proj,
    filter_decay, skip_gain, w_out,
):
    rows, cols = lax.axis_size("row"), lax.axis_size("col")
    tok_rows = tokens.shape[1]
    chan_col = w_value.shape[1]
    chans = chan_col // rows
    groups = chans // PACK
    length = tok_rows * rows
    block_q = tok_rows // LANES
    length_q = length // LANES
    width = tok_rows // cols
    depth = w_out.shape[1]
    emb, hid = filter_embed.shape
    half = length_q + 1

    flat = tokens.reshape(tok_rows, tokens.shape[2])
    bands = (emb - 1) // 2
    index = np.arange(length)
    spot = index.astype(np.float32) / np.float32(length - 1)
    phase = 2.0 * np.pi * (np.outer(np.arange(1, bands + 1), index) % length) / length
    features = np.concatenate([spot[None, :], np.cos(phase), np.sin(phase)])
    emb_pad = -(-emb // 8) * 8
    features = np.concatenate([features, np.zeros((emb_pad - emb, length))]).astype(np.float32).astype(np.float64)
    high, middle, least = host_split(features)
    features = np.concatenate([high, middle, high, least, middle, high]).astype(jnp.bfloat16.dtype)
    own = np.arange(chan_col).reshape(rows, groups, PACK).transpose(1, 0, 2).reshape(-1)
    perm = np.zeros((chan_col, chan_col), np.float32)
    perm[own, np.arange(chan_col)] = 1.0
    lanes = chan_col // LANES
    fproj = filter_proj.reshape(hid, 2, 2, lanes, LANES).transpose(0, 1, 3, 2, 4).reshape(hid * 4 * lanes, LANES)
    w_rows = w_out.reshape(rows, groups, PACK, depth)

    first, last, twist, ahead, back = dft_tables(length)
    operands = (
        flat, w_value, w_first, w_second, w_gate, w_rows, conv_taps, filter_embed, filter_freq.reshape(1, hid),
        fproj, filter_decay, skip_gain, jnp.asarray(features), first, last, twist, ahead, back,
        jnp.asarray(perm).astype(jnp.bfloat16),
    )
    dma = pltpu.SemaphoreType.DMA
    f32, low = jnp.float32, jnp.bfloat16
    like = lambda array: pltpu.VMEM(array.shape, array.dtype)
    mixed = pl.pallas_call(
        functools.partial(mixer_kernel, rows, cols, width, emb),
        out_shape=jax.ShapeDtypeStruct((width, depth), low),
        in_specs=[pl.BlockSpec(memory_space=pl.ANY)] * len(operands),
        out_specs=pl.BlockSpec(memory_space=pltpu.VMEM),
        scratch_shapes=[
            like(flat),
            pltpu.VMEM((4,) + w_value.shape, low),
            like(conv_taps),
            pltpu.VMEM((emb_pad, hid), f32),
            pltpu.VMEM((1, hid), f32),
            like(fproj),
            like(filter_decay),
            like(skip_gain),
            pltpu.VMEM(features.shape, low),
            like(first),
            like(last),
            like(twist),
            like(ahead),
            like(back),
            pltpu.VMEM(perm.shape, low),
            pltpu.VMEM((2, rows, groups, block_q, PACK, LANES), low),
            pltpu.VMEM((2, rows, groups, block_q, PACK, LANES), low),
            pltpu.VMEM((2, 2, groups * half * PACK, LANES), f32),
            pltpu.VMEM((4, chans, length), low),
            pltpu.VMEM((16, chan_col), f32),
            pltpu.VMEM((8, groups, PACK, LANES), f32),
            pltpu.VMEM((cols, groups, width, rows * PACK), low),
            pltpu.VMEM((cols, groups, width, rows * PACK), low),
            pltpu.VMEM((2, 8, chan_col), f32),
            pltpu.VMEM((2, 8, chan_col), f32),
            pltpu.VMEM((length_q, groups, PACK, LANES), low),
            pltpu.VMEM((cols, rows, PACK, LANES), low),
            pltpu.VMEM((cols, rows, groups, PACK, depth), low),
            dma((len(operands),)),
            dma((2, rows - 1)),
            dma((2, rows - 1)),
            dma((2,)),
            dma((2,)),
            dma((cols - 1,)),
            dma((cols - 1,)),
            dma((rows * cols - 1,)),
            dma((rows * cols - 1,)),
            dma((4,)),
            dma((4,)),
            dma((2,)),
            dma((2,)),
            dma((2 * cols - 2,)),
            dma((2 * cols - 2,)),
        ],
        compiler_params=pltpu.CompilerParams(
            collective_id=0, has_side_effects=True, vmem_limit_bytes=60 * 1024 * 1024
        ),
        cost_estimate=pl.CostEstimate(flops=12_000_000_000, bytes_accessed=8_000_000, transcendentals=0),
    )(*operands)
    return mixed[None]


def shaped_body(tokens, w_value, *rest):
    rows, cols = lax.axis_size("row"), lax.axis_size("col")
    seqs, tok_rows = tokens.shape[:2]
    chan_col = w_value.shape[1]
    chans = chan_col // rows
    width = tok_rows // cols
    fits = (
        seqs == 1
        and cols == 4
        and rows == 8
        and chans == 2 * PACK
        and tok_rows % LANES == 0
        and LANES == 2 * width
        and chan_col == 2 * LANES
        and rows * PACK == LANES
    )
    return (fast_body if fits else body)(tokens, w_value, *rest)


def solution(mesh):
    in_specs = (
        P(None, "row", None),
        P(None, "col"),
        P(None, "col"),
        P(None, "col"),
        P(None, "col"),
        P(None, None, "col"),
        P(),
        P(),
        P(None, None, None, "col"),
        P(None, None, "col"),
        P(None, "col"),
        P("col", None),
    )
    out_specs = P(None, ("row", "col"), None)
    return jax.shard_map(shaped_body, mesh=mesh, in_specs=in_specs, out_specs=out_specs, check_vma=False)
```

time: 52.6 us -> 33.6 us (0.64)
  the two profiles are of different devices: /device:TPU:0 before, /device:TPU:1 now
where the time goes in v1:
time: 33.6 us; the launch traced here: 33.4 us
  Pallas kernels  31.8 us (95%)
  local copies, waits for them, and re-layouts  1.67 us (5%)
    pallas_call x1, Pallas kernels, fast_body(): pl.pallas_call(functools.partial(mixer_kernel, rows, cols, width, emb), o...  31.8 us
    unnamed x1, local copies, waits for them, and re-layouts  1.67 us

profile of v1, /device:TPU:1, one launch (start us, length us, event | category | flops | bytes accessed | tf_op | source)
XLA Modules:
  0.0 33.4 jit_solution(11956536658705397875)
XLA Ops:
  0.0 31.8 %shard_map.181 = bf16[64,2048]{1,0:T(8,128)(2,1)} custom-call(bf16[256,2048]{1,0:T(8,128)(2,1)} %bitcast.10, bf16[2048,256]{1,0:T(8,128)(2,1)} %w_value_hbm.1, bf16[2048,256]{1,0:T(8,128)(2,1)} %w_first_hbm.1, bf16[2048,256]{1,0:T(8,128)(2,1)} %w_second_hbm.1, bf16[2048,256]{1,0:T(8,128)(2,1)} %w_gate_hbm.1, bf16[8,2,16,2048]{3,2,1,0:T(8,128)(2,1)} %bitcast.11, ...), custom_call_target="tpu_custom_call" | custom-call | flops 12000000000 | bytes 8000000 | tf_op jit(solution)/shard_map/pallas_call | solution.py:679
  31.8 1.7 %copy.22 = bf16[1,64,2048]{2,1,0:T(8,128)(2,1)} copy(bf16[1,64,2048]{2,1,0:T(8,128)(2,1)} %bitcast.9) | data formatting | bytes 524288

commit v2 on v1

--- a/solution.py
+++ b/solution.py
@@ -263,9 +263,9 @@
     out_ref,
     tokens_ref, w_refs, conv_ref, embed_ref, freq_ref, fproj_ref, decay_ref, gain_ref, features_ref, first_ref,
     last_ref, twist_ref, ahead_ref, back_ref, perm_ref,
-    send, recv, spectra, taps_ref, stack_ref, coef_ref, gated, gated_in, edge_out, edge_in, piece, final, weights,
+    send, recv, spectra, taps_ref, stack_ref, coef_ref, gated, gated_in, edge_out, edge_in, piece, final, weights, total,
     load_sem, row_send, row_recv, edge_send, edge_recv, gate_send, gate_recv, piece_send, piece_recv,
-    wide_send, wide_recv, pass_send, pass_recv, mate_send, mate_recv,
+    wide_send, wide_recv, level_send, level_recv, pass_send, pass_recv, mate_send, mate_recv, told,
 ):
     my_row = lax.axis_index("row")
     my_col = lax.axis_index("col")
@@ -286,11 +286,31 @@
             device_id=(row, col), device_id_type=mesh_id,
         )
 
+    side = lax.rem(my_row, 2)
+    mate = flip(my_row, 1)
+    low_row = my_row - side
     barrier = pltpu.get_barrier_semaphore()
-    for d in range(1, rows):
-        pl.semaphore_signal(barrier, inc=1, device_id=(flip(my_row, d), my_col), device_id_type=mesh_id)
+
+    def greet(row, col):
+        pl.semaphore_signal(barrier, inc=1, device_id=(row, col), device_id_type=mesh_id)
+
+    greet(mate, my_col)
     for d in range(1, cols):
-        pl.semaphore_signal(barrier, inc=1, device_id=(my_row, flip(my_col, d)), device_id_type=mesh_id)
+        greet(low_row, flip(my_col, d))
+    for d in range(1, rows // 2):
+        greet(flip(low_row, 2 * d) + 1, my_col)
+
+    def heard(own_side):
+        others = 2 * cols - 1 if own_side == 0 else rows - 1
+
+        @pl.when(side == own_side)
+        def _():
+            pl.semaphore_wait(barrier, others)
+            pl.semaphore_signal(told, inc=1, device_id=(mate, my_col), device_id_type=mesh_id)
+
+        @pl.when(side != own_side)
+        def _():
+            pl.semaphore_wait(told, 1)
 
     loads = {}
     for name, src, dst in (
@@ -317,30 +337,50 @@
         loads[name] = pltpu.make_async_copy(src, dst, load_sem.at[len(loads)])
         loads[name].start()
 
-    side = lax.rem(my_row, 2)
-    mate = flip(my_row, 1)
-    quarter = rows // 4
-    rows_of = lambda part: pl.ds(side * (rows // 2) + part * quarter, quarter)
-
-    def wide_copy(index, d, part):
+    plane = lax.rem(lax.div(my_row, 2), 2)
+    subs = rows // 2
+    row_of = lambda sub: side * subs + sub
+
+    def wide_copy(index, d, sub):
         return remote(
-            w_out_hbm.at[rows_of(part)], weights.at[d, rows_of(part)],
+            w_out_hbm.at[row_of(sub)], weights.at[d, row_of(sub)],
             wide_send.at[index], wide_recv.at[index], my_row, flip(my_col, d),
         )
 
-    wide = {(1, 0): wide_copy(0, 1, 0), (2, 1): wide_copy(1, 2, 1), (1, 1): wide_copy(2, 1, 1), (2, 0): wide_copy(3, 2, 0)}
-    passed = {
-        0: remote(weights.at[1, rows_of(0)], weights.at[3, rows_of(0)], pass_send.at[0], pass_recv.at[0], my_row, flip(my_col, 2)),
-        1: remote(weights.at[2, rows_of(1)], weights.at[3, rows_of(1)], pass_send.at[1], pass_recv.at[1], my_row, flip(my_col, 1)),
+    wide = {
+        (d, sub): wide_copy(index, d, sub + plane if sub == mixed else sub)
+        for index, (d, sub, mixed) in enumerate(
+            ((1, 0, 0), (2, 2, 2), (1, 2, 0), (2, 0, 2), (1, 3, 0), (2, 1, 2))
+        )
     }
+
+    def level_copy(index, d, sub):
+        part = weights.at[d, row_of(sub + plane)]
+        return remote(part, part, level_send.at[index], level_recv.at[index], flip(my_row, 2), my_col)
+
+    level = {1: level_copy(0, 1, 0), 2: level_copy(1, 2, 2)}
+
+    def pass_copy(index, d, sub):
+        return remote(
+            weights.at[d, row_of(sub)], weights.at[3, row_of(sub)],
+            pass_send.at[index], pass_recv.at[index], my_row, flip(my_col, 3 - d),
+        )
+
+    passed = {(d, sub): pass_copy(i, d, sub) for i, (d, sub) in enumerate(((1, 2), (2, 0), (1, 3), (2, 1)))}
+
+    def mate_copy(index, d, sub):
+        part = weights.at[d, row_of(sub)]
+        return remote(part, part, mate_send.at[index], mate_recv.at[index], mate, my_col)
+
     mates = {}
     for d in range(1, cols):
-        for part in range(2):
-            index = 2 * (d - 1) + part
-            mates[d, part] = remote(
-                weights.at[d, rows_of(part)], weights.at[d, rows_of(part)],
-                mate_send.at[index], mate_recv.at[index], mate, my_col,
-            )
+        for sub in range(subs):
+            here = sub
+            if d == 1 and sub < 2:
+                here = plane if sub == 0 else 1 - plane
+            if d == 2 and sub >= 2:
+                here = 2 + plane if sub == 2 else 3 - plane
+            mates[d, sub] = mate_copy(subs * (d - 1) + sub, d, here)
 
     far_first = sorted(range(1, rows), key=lambda d: -(d & (rows // 2)))
 
@@ -365,21 +405,16 @@
 
     value_copies, first_copies = row_copies(0), row_copies(1)
 
+    heard(0)
+    for copy in wide.values():
+        copy.start()
     loads["tokens"].wait()
     loads["value"].wait()
     project_turned(0)
-    pl.semaphore_wait(barrier, rows + cols - 2)
+    heard(1)
     for copy in value_copies:
         copy.start()
-    wide[1, 0].start()
-    wide[2, 1].start()
     recv[0, my_row] = send[0, my_row]
-
-    loads["first"].wait()
-    project_turned(1)
-    for copy in first_copies:
-        copy.start()
-    recv[1, my_row] = send[1, my_row]
 
     loads["second"].wait()
     second = project(2).astype(low).astype(f32)
@@ -391,6 +426,11 @@
     ]
     for copy in edges:
         copy.start()
+    loads["first"].wait()
+    project_turned(1)
+    for copy in first_copies:
+        copy.start()
+    recv[1, my_row] = send[1, my_row]
     loads["gate"].wait()
     gate = project(3).astype(low).astype(f32)
     loads["conv"].wait()
@@ -520,6 +560,34 @@
                 spectra[order, 0] += spec[:, :LANES]
                 spectra[order, 1] -= spec[:, LANES:]
 
+    for d in (1, 2):
+        wide[d, 2 * d - 2].wait_recv()
+        level[d].start()
+        mates[d, 2 * d - 2].start()
+
+    def short(role):
+        blocks = []
+        for g in range(groups):
+            here = recv[role, :, g].reshape(length_q * PACK, LANES).astype(f32)
+            size = here.shape[0]
+            lane = lax.broadcasted_iota(jnp.int32, here.shape, 1)
+            blank = jnp.zeros((PACK, LANES), f32)
+            before = pltpu.roll(here, 1, 1)
+            before = jnp.where(lane == 0, jnp.concatenate([blank, before[: size - PACK]], axis=0), before)
+            after = pltpu.roll(here, LANES - 1, 1)
+            after = jnp.where(lane == LANES - 1, jnp.concatenate([after[PACK:], blank], axis=0), after)
+            shape = (length_q, PACK, LANES)
+            w = lambda j: coef_ref[3 * role + j, g][None]
+            result = before.reshape(shape) * w(0) + here.reshape(shape) * w(1) + after.reshape(shape) * w(2)
+            blocks.append(result.reshape(size, LANES))
+        return jnp.concatenate(blocks, axis=1)
+
+    loads["back"].wait()
+    loads["dft_last"].wait()
+    for copy in value_copies:
+        copy.wait_recv()
+    conv = convolve(short(0), 0)
+
     for copy in edges:
         copy.wait_recv()
     line = lax.broadcasted_iota(jnp.int32, second.shape, 0)
@@ -543,31 +611,7 @@
     for copy in gate_copies:
         copy.start()
     gated_in[0] = gated[my_col]
-    wide[1, 1].start()
-    wide[2, 0].start()
-
-    def short(role):
-        blocks = []
-        for g in range(groups):
-            here = recv[role, :, g].reshape(length_q * PACK, LANES).astype(f32)
-            size = here.shape[0]
-            lane = lax.broadcasted_iota(jnp.int32, here.shape, 1)
-            blank = jnp.zeros((PACK, LANES), f32)
-            before = pltpu.roll(here, 1, 1)
-            before = jnp.where(lane == 0, jnp.concatenate([blank, before[: size - PACK]], axis=0), before)
-            after = pltpu.roll(here, LANES - 1, 1)
-            after = jnp.where(lane == LANES - 1, jnp.concatenate([after[PACK:], blank], axis=0), after)
-            shape = (length_q, PACK, LANES)
-            w = lambda j: coef_ref[3 * role + j, g][None]
-            result = before.reshape(shape) * w(0) + here.reshape(shape) * w(1) + after.reshape(shape) * w(2)
-            blocks.append(result.reshape(size, LANES))
-        return jnp.concatenate(blocks, axis=1)
-
-    loads["back"].wait()
-    loads["dft_last"].wait()
-    for copy in value_copies:
-        copy.wait_recv()
-    conv = convolve(short(0), 0)
+
     for copy in first_copies:
         copy.wait_recv()
     conv = convolve(short(1) * conv, 1)
@@ -594,41 +638,41 @@
         copy.start()
     final[0, my_row] = piece[my_row * block_q + lax.div(my_col, 2), lax.rem(my_col, 2)]
 
-    wide[1, 0].wait_recv()
-    passed[0].start()
-    mates[1, 0].start()
-    wide[2, 1].wait_recv()
-    passed[1].start()
-    mates[2, 1].start()
-    wide[1, 1].wait_recv()
-    mates[1, 1].start()
-    wide[2, 0].wait_recv()
-    mates[2, 0].start()
-    for part in range(2):
-        passed[part].wait_recv()
-        mates[3, part].start()
+    for key, copy in passed.items():
+        wide[key].wait_recv()
+        copy.start()
+        mates[key].start()
+    for d in (1, 2):
+        level[d].wait_recv()
+        mates[d, 2 * d - 1].start()
 
     for copy in gate_copies:
         copy.wait_recv()
     for copy in piece_copies:
         copy.wait_recv()
     loads["w_out"].wait()
-    picked = []
-    for d in range(cols):
+    depth = weights.shape[4]
+
+    def share(d):
         outer = final[d].reshape(rows * PACK, LANES).astype(f32).T
         outer = (outer * gated_in[d].reshape(groups * width, per_group).astype(f32)).astype(low)
-        for g in range(groups):
-            picked.append(outer[g * width : (g + 1) * width])
-    for copy in mates.values():
-        copy.wait_recv()
-    depth = weights.shape[4]
-    full = jnp.concatenate(
-        [weights[d, :, g].reshape(per_group, depth) for d in range(cols) for g in range(groups)], axis=0
-    )
-    out_ref[...] = jnp.dot(jnp.concatenate(picked, axis=1), full, preferred_element_type=f32).astype(low)
+        left = jnp.concatenate([outer[g * width : (g + 1) * width] for g in range(groups)], axis=1)
+        right = jnp.concatenate([weights[d, :, g].reshape(per_group, depth) for g in range(groups)], axis=0)
+        return jnp.dot(left, right, preferred_element_type=f32)
+
+    for d in (1, 2):
+        for sub in range(subs):
+            mates[d, sub].wait_recv()
+    total[...] = share(0) + share(1) + share(2)
+    for d, sub in ((2, 0), (1, 2), (2, 1), (1, 3)):
+        passed[d, sub].wait_recv()
+        mates[3, sub].start()
+    for sub in range(subs):
+        mates[3, sub].wait_recv()
+    out_ref[...] = (total[...] + share(3)).astype(low)
     for copy in value_copies + first_copies + edges + gate_copies + piece_copies:
         copy.wait_send()
-    for group in (wide, passed, mates):
+    for group in (wide, level, passed, mates):
         for copy in group.values():
             copy.wait_send()
 
@@ -678,7 +722,7 @@
     like = lambda array: pltpu.VMEM(array.shape, array.dtype)
     mixed = pl.pallas_call(
         functools.partial(mixer_kernel, rows, cols, width, emb),
-        out_shape=jax.ShapeDtypeStruct((width, depth), low),
+        out_shape=pltpu.VMEM((width, depth), low),
         in_specs=[pl.BlockSpec(memory_space=pl.ANY)] * len(operands),
         out_specs=pl.BlockSpec(memory_space=pltpu.VMEM),
         scratch_shapes=[
@@ -710,6 +754,7 @@
             pltpu.VMEM((length_q, groups, PACK, LANES), low),
             pltpu.VMEM((cols, rows, PACK, LANES), low),
             pltpu.VMEM((cols, rows, groups, PACK, depth), low),
+            pltpu.VMEM((width, depth), f32),
             dma((len(operands),)),
             dma((2, rows - 1)),
             dma((2, rows - 1)),
@@ -719,18 +764,21 @@
             dma((cols - 1,)),
             dma((rows * cols - 1,)),
             dma((rows * cols - 1,)),
+            dma((6,)),
+            dma((6,)),
+            dma((2,)),
+            dma((2,)),
             dma((4,)),
             dma((4,)),
-            dma((2,)),
-            dma((2,)),
-            dma((2 * cols - 2,)),
-            dma((2 * cols - 2,)),
+            dma(((cols - 1) * rows // 2,)),
+            dma(((cols - 1) * rows // 2,)),
+            pltpu.SemaphoreType.REGULAR,
         ],
         compiler_params=pltpu.CompilerParams(
-            collective_id=0, has_side_effects=True, vmem_limit_bytes=60 * 1024 * 1024
+            collective_id=0, has_side_effects=True, vmem_limit_bytes=40 * 1024 * 1024
         ),
         cost_estimate=pl.CostEstimate(flops=12_000_000_000, bytes_accessed=8_000_000, transcendentals=0),
-    )(*operands)
+    )(*[pltpu.with_memory_space_constraint(array, pltpu.HBM) for array in operands])
     return mixed[None]
 
 

time: 33.6 us -> 27.4 us (0.82)
  the two profiles are of different devices: /device:TPU:1 before, /device:TPU:0 now
where the time goes in v2:
time: 27.4 us; the launch traced here: 26.9 us
  Pallas kernels  26.2 us (96%)
  local copies, waits for them, and re-layouts  0.71 us (3%)
    pallas_call x1, Pallas kernels, fast_body(): pl.pallas_call(functools.partial(mixer_kernel, rows, cols, width, emb), o...  26.2 us
    unnamed x1, local copies, waits for them, and re-layouts  0.71 us

profile of v2, /device:TPU:0, one launch (start us, length us, event | category | flops | bytes accessed | tf_op | source)
XLA Modules:
  0.0 26.9 jit_solution(3094475541766654379)
XLA Ops:
  0.0 26.2 %shard_map.181 = bf16[64,2048]{1,0:T(8,128)(2,1)S(1)} custom-call(bf16[256,2048]{1,0:T(8,128)(2,1)} %bitcast.10, bf16[2048,256]{1,0:T(8,128)(2,1)} %w_value_hbm.1, bf16[2048,256]{1,0:T(8,128)(2,1)} %w_first_hbm.1, bf16[2048,256]{1,0:T(8,128)(2,1)} %w_second_hbm.1, bf16[2048,256]{1,0:T(8,128)(2,1)} %w_gate_hbm.1, bf16[8,2,16,2048]{3,2,1,0:T(8,128)(2,1)} %bitcast.11, ...), custom_call_target="tpu_custom_call" | custom-call | flops 12000000000 | bytes 8000000 | tf_op jit(solution)/shard_map/pallas_call | solution.py:723
  26.2 0.7 %copy.22 = bf16[1,64,2048]{2,1,0:T(8,128)(2,1)} copy(bf16[1,64,2048]{2,1,0:T(8,128)(2,1)S(1)} %bitcast.9) | data formatting | bytes 524288

commit v3 on v2

--- a/solution.py
+++ b/solution.py
@@ -228,8 +228,7 @@
     cos, sin = np.cos(angle), np.sin(angle)
     ahead = np.block([[cos, -sin], [sin, cos]])
     back = np.block([[cos, sin], [-sin, cos]])
-    low = lambda array: jnp.asarray(array.astype(np.float32)).astype(jnp.bfloat16)
-    return low(first), low(last), jnp.asarray(twist.astype(np.float32)), low(ahead), low(back)
+    return first, last, jnp.asarray(twist.astype(np.float32)), ahead, back
 
 
 def split_bf16(array):
@@ -259,13 +258,13 @@
 def mixer_kernel(
     rows, cols, width, emb,
     tokens_hbm, w_value_hbm, w_first_hbm, w_second_hbm, w_gate_hbm, w_out_hbm, conv_hbm, embed_hbm, freq_hbm,
-    proj_hbm, decay_hbm, gain_hbm, features_hbm, first_hbm, last_hbm, twist_hbm, ahead_hbm, back_hbm, perm_hbm,
+    proj_hbm, decay_hbm, gain_hbm, features_hbm, tables_hbm, twist_hbm,
     out_ref,
-    tokens_ref, w_refs, conv_ref, embed_ref, freq_ref, fproj_ref, decay_ref, gain_ref, features_ref, first_ref,
-    last_ref, twist_ref, ahead_ref, back_ref, perm_ref,
+    tokens_ref, w_refs, conv_ref, embed_ref, freq_ref, fproj_ref, decay_ref, gain_ref, features_ref, tables_ref,
+    twist_ref,
     send, recv, spectra, taps_ref, stack_ref, coef_ref, gated, gated_in, edge_out, edge_in, piece, final, weights, total,
     load_sem, row_send, row_recv, edge_send, edge_recv, gate_send, gate_recv, piece_send, piece_recv,
-    wide_send, wide_recv, level_send, level_recv, pass_send, pass_recv, mate_send, mate_recv, told,
+    wide_send, wide_recv, level_send, level_recv, pass_send, pass_recv, mate_send, mate_recv, told, ready,
 ):
     my_row = lax.axis_index("row")
     my_col = lax.axis_index("col")
@@ -278,6 +277,7 @@
     length = tok_rows * rows
     half = length_q + 1
     hid = freq_ref.shape[1]
+    depth = weights.shape[4]
     f32, low = jnp.float32, jnp.bfloat16
 
     def remote(src, dst, send_sem, recv_sem, row, col):
@@ -294,14 +294,15 @@
     def greet(row, col):
         pl.semaphore_signal(barrier, inc=1, device_id=(row, col), device_id_type=mesh_id)
 
+    near = (1, 2)
     greet(mate, my_col)
-    for d in range(1, cols):
+    for d in near:
         greet(low_row, flip(my_col, d))
     for d in range(1, rows // 2):
         greet(flip(low_row, 2 * d) + 1, my_col)
 
     def heard(own_side):
-        others = 2 * cols - 1 if own_side == 0 else rows - 1
+        others = 2 * len(near) + 1 if own_side == 0 else rows - 1
 
         @pl.when(side == own_side)
         def _():
@@ -312,30 +313,30 @@
         def _():
             pl.semaphore_wait(told, 1)
 
+    def await_bytes(ref, sem):
+        pltpu.make_async_copy(ref, ref, sem).wait()
+
+    token_sem, weight_sem = load_sem.at[0], load_sem.at[1]
+    pltpu.make_async_copy(tokens_hbm, tokens_ref, token_sem).start()
+    pltpu.make_async_copy(w_value_hbm, w_refs.at[0], token_sem).start()
     loads = {}
     for name, src, dst in (
-        ("tokens", tokens_hbm, tokens_ref),
-        ("value", w_value_hbm, w_refs.at[0]),
         ("embed", embed_hbm, embed_ref.at[pl.ds(0, emb)]),
         ("freq", freq_hbm, freq_ref),
         ("conv", conv_hbm, conv_ref),
         ("gain", gain_hbm, gain_ref),
         ("decay", decay_hbm, decay_ref),
-        ("first", w_first_hbm, w_refs.at[1]),
-        ("second", w_second_hbm, w_refs.at[2]),
-        ("gate", w_gate_hbm, w_refs.at[3]),
         ("fproj", proj_hbm, fproj_ref),
         ("features", features_hbm, features_ref),
-        ("dft_first", first_hbm, first_ref),
+        ("tables", tables_hbm, tables_ref),
         ("twist", twist_hbm, twist_ref),
-        ("ahead", ahead_hbm, ahead_ref),
-        ("perm", perm_hbm, perm_ref),
-        ("back", back_hbm, back_ref),
-        ("dft_last", last_hbm, last_ref),
         ("w_out", w_out_hbm, weights.at[0]),
     ):
-        loads[name] = pltpu.make_async_copy(src, dst, load_sem.at[len(loads)])
-        loads[name].start()
+        loads[name] = pltpu.make_async_copy(src, dst, load_sem.at[2 + len(loads)])
+    for role, w_hbm in ((2, w_second_hbm), (1, w_first_hbm), (3, w_gate_hbm)):
+        pltpu.make_async_copy(w_hbm, w_refs.at[role], weight_sem).start()
+    for copy in loads.values():
+        copy.start()
 
     plane = lax.rem(lax.div(my_row, 2), 2)
     subs = rows // 2
@@ -344,43 +345,47 @@
     def wide_copy(index, d, sub):
         return remote(
             w_out_hbm.at[row_of(sub)], weights.at[d, row_of(sub)],
-            wide_send.at[index], wide_recv.at[index], my_row, flip(my_col, d),
+            wide_send, wide_recv.at[index // 2], my_row, flip(my_col, d),
         )
 
     wide = {
         (d, sub): wide_copy(index, d, sub + plane if sub == mixed else sub)
         for index, (d, sub, mixed) in enumerate(
-            ((1, 0, 0), (2, 2, 2), (1, 2, 0), (2, 0, 2), (1, 3, 0), (2, 1, 2))
+            ((1, 0, 0), (2, 2, 2), (1, 3, 0), (2, 1, 2), (1, 2, 0), (2, 0, 2))
         )
     }
 
-    def level_copy(index, d, sub):
-        part = weights.at[d, row_of(sub + plane)]
-        return remote(part, part, level_send.at[index], level_recv.at[index], flip(my_row, 2), my_col)
-
-    level = {1: level_copy(0, 1, 0), 2: level_copy(1, 2, 2)}
-
-    def pass_copy(index, d, sub):
+    def there(part, send_sem, recv_sem, row):
+        return remote(part, part, send_sem, recv_sem, row, my_col)
+
+    own_half, far_half = pl.ds(plane, 1), pl.ds(1 - plane, 1)
+    all_of = pl.ds(0, groups)
+    level_row = flip(my_row, 2)
+    level = {
+        d: there(weights.at[d, row_of(2 * d - 2 + plane)], level_send, level_recv.at[0], level_row) for d in (1, 2)
+    }
+    level_late = {
+        sub: there(weights.at[3, row_of(sub), own_half, pl.ds(0, PACK), pl.ds(0, depth // 2)], level_send, level_recv.at[1], level_row) for sub in (3, 1)
+    }
+
+    shared, unshared = pl.ds(0, depth // 2), pl.ds(depth // 2, depth // 2)
+    every_row, every_lane = pl.ds(0, PACK), pl.ds(0, depth)
+
+    def pass_copy(index, d, sub, span, lanes):
         return remote(
-            weights.at[d, row_of(sub)], weights.at[3, row_of(sub)],
-            pass_send.at[index], pass_recv.at[index], my_row, flip(my_col, 3 - d),
+            weights.at[d, row_of(sub), span, every_row, lanes], weights.at[3, row_of(sub), span, every_row, lanes],
+            pass_send, pass_recv.at[index], my_row, flip(my_col, 3 - d),
         )
 
-    passed = {(d, sub): pass_copy(i, d, sub) for i, (d, sub) in enumerate(((1, 2), (2, 0), (1, 3), (2, 1)))}
-
-    def mate_copy(index, d, sub):
-        part = weights.at[d, row_of(sub)]
-        return remote(part, part, mate_send.at[index], mate_recv.at[index], mate, my_col)
-
-    mates = {}
-    for d in range(1, cols):
-        for sub in range(subs):
-            here = sub
-            if d == 1 and sub < 2:
-                here = plane if sub == 0 else 1 - plane
-            if d == 2 and sub >= 2:
-                here = 2 + plane if sub == 2 else 3 - plane
-            mates[d, sub] = mate_copy(subs * (d - 1) + sub, d, here)
+    passed = {
+        (1, 3): [pass_copy(0, 1, 3, own_half, shared), pass_copy(3, 1, 3, all_of, unshared)],
+        (2, 1): [pass_copy(0, 2, 1, own_half, shared), pass_copy(3, 2, 1, all_of, unshared)],
+        (1, 2): [pass_copy(1, 1, 2, all_of, every_lane)],
+        (2, 0): [pass_copy(2, 2, 0, all_of, every_lane)],
+    }
+
+    def to_mate(d, sub, span=all_of, lanes=every_lane):
+        there(weights.at[d, row_of(sub), span, every_row, lanes], mate_send, mate_recv.at[d // 3], mate).start()
 
     far_first = sorted(range(1, rows), key=lambda d: -(d & (rows // 2)))
 
@@ -388,7 +393,7 @@
         return [
             remote(
                 send.at[role, flip(my_row, d)], recv.at[role, my_row],
-                row_send.at[role, d - 1], row_recv.at[role, d - 1], flip(my_row, d), my_col,
+                row_send.at[role], row_recv.at[role], flip(my_row, d), my_col,
             )
             for d in far_first
         ]
@@ -408,30 +413,34 @@
     heard(0)
     for copy in wide.values():
         copy.start()
-    loads["tokens"].wait()
-    loads["value"].wait()
+    await_bytes(w_refs.at[pl.ds(0, 2)], token_sem)
     project_turned(0)
     heard(1)
     for copy in value_copies:
         copy.start()
     recv[0, my_row] = send[0, my_row]
 
-    loads["second"].wait()
+    await_bytes(w_refs.at[pl.ds(1, 3)], weight_sem)
     second = project(2).astype(low).astype(f32)
     edge_out[0] = jnp.broadcast_to(second[tok_rows - 1 :], edge_out.shape[1:])
     edge_out[1] = jnp.broadcast_to(second[:1], edge_out.shape[1:])
-    edges = [
-        remote(edge_out.at[0], edge_in.at[0], edge_send.at[0], edge_recv.at[0], lax.rem(my_row + 1, rows), my_col),
-        remote(edge_out.at[1], edge_in.at[1], edge_send.at[1], edge_recv.at[1], lax.rem(my_row + rows - 1, rows), my_col),
-    ]
-    for copy in edges:
-        copy.start()
-    loads["first"].wait()
+    def edge_copy(index, step):
+        return remote(edge_out.at[index], edge_in.at[index], edge_send.at[index], edge_recv.at[index], my_row + step, my_col)
+
+    has_above, has_below = my_row > 0, my_row < rows - 1
+
+    @pl.when(has_below)
+    def _():
+        edge_copy(0, 1).start()
+
+    @pl.when(has_above)
+    def _():
+        edge_copy(1, -1).start()
+
     project_turned(1)
     for copy in first_copies:
         copy.start()
     recv[1, my_row] = send[1, my_row]
-    loads["gate"].wait()
     gate = project(3).astype(low).astype(f32)
     loads["conv"].wait()
 
@@ -488,6 +497,12 @@
             block = jnp.where(lag == 0, 0.0, block)
         taps_ref[od] = block.astype(low)
 
+    size = LANES * groups
+    first_ref, last_ref, ahead_ref, back_ref, perm_ref = (
+        tables_ref.at[pl.ds(start * size, count * size)]
+        for start, count in ((0, 2), (2, 2), (4, 1), (5, 1), (6, 1))
+    )
+
     def wide_twist(index):
         return twist_ref[index].reshape(half, 1, 8, LANES)
 
@@ -528,14 +543,14 @@
             turned_real = (real * cos - imag * sin).reshape(half * PACK, LANES)
             turned_imag = (real * sin + imag * cos)[1:-1].reshape((half - 2) * PACK, LANES)
             blocks.append(jnp.concatenate([turned_real, turned_imag], axis=0).astype(low))
-        result = jnp.dot(last_ref[...], jnp.concatenate(blocks, axis=1), preferred_element_type=f32)
+        last = jnp.concatenate([last_ref[:size], last_ref[size:]], axis=1)
+        result = jnp.dot(last, jnp.concatenate(blocks, axis=1), preferred_element_type=f32)
         gain = jnp.concatenate([coef_ref[6 + order, g] for g in range(groups)], axis=1)
         shape = (length_q, PACK, groups * LANES)
         return (result.reshape(shape) + gain[None] * signal.reshape(shape)).reshape(signal.shape)
 
-    loads["dft_first"].wait()
+    loads["tables"].wait()
     loads["twist"].wait()
-    loads["ahead"].wait()
     for order in range(2):
         for direction in range(2):
             od = 2 * order + direction
@@ -560,10 +575,47 @@
                 spectra[order, 0] += spec[:, :LANES]
                 spectra[order, 1] -= spec[:, LANES:]
 
+    await_bytes(weights.at[0, pl.ds(0, 2)], wide_recv.at[0])
     for d in (1, 2):
-        wide[d, 2 * d - 2].wait_recv()
         level[d].start()
-        mates[d, 2 * d - 2].start()
+        to_mate(d, 2 * d - 2 + plane)
+
+
+    @pl.when(has_above)
+    def _():
+        await_bytes(edge_in.at[0], edge_recv.at[0])
+
+    @pl.when(has_below)
+    def _():
+        await_bytes(edge_in.at[1], edge_recv.at[1])
+
+    line = lax.broadcasted_iota(jnp.int32, second.shape, 0)
+    above = jnp.where(has_above, edge_in[0, 0:1], 0.0)
+    below = jnp.where(has_below, edge_in[1, 0:1], 0.0)
+    before = jnp.where(line == 0, above, pltpu.roll(second, 1, 0))
+    after = jnp.where(line == tok_rows - 1, below, pltpu.roll(second, tok_rows - 1, 0))
+    short_second = before * conv_ref[0, 2:3] + second * conv_ref[1, 2:3] + after * conv_ref[2, 2:3]
+    both = (short_second * (gate / (1.0 + jnp.exp(-gate)))).astype(low)
+    both = jnp.dot(both, perm_ref[...], preferred_element_type=f32).astype(low)
+    per_group = rows * PACK
+    for g in range(groups):
+        gated[:, g] = both[:, g * per_group : (g + 1) * per_group].reshape(cols, width, per_group)
+    gate_copies = [
+        remote(
+            gated.at[flip(my_col, d)], gated_in.at[d], gate_send, gate_recv, my_row, flip(my_col, d)
+        )
+        for d in range(1, cols)
+    ]
+    for copy in gate_copies:
+        copy.start()
+    gated_in[0] = gated[my_col]
+
+    def pass_on(index, keys):
+        await_bytes(weights.at[0, pl.ds(0, 2)], wide_recv.at[1 + index])
+        for key in keys:
+            for copy in passed[key]:
+                copy.start()
+            to_mate(*key)
 
     def short(role):
         blocks = []
@@ -582,38 +634,13 @@
             blocks.append(result.reshape(size, LANES))
         return jnp.concatenate(blocks, axis=1)
 
-    loads["back"].wait()
-    loads["dft_last"].wait()
-    for copy in value_copies:
-        copy.wait_recv()
+    others = pl.ds(0, rows - 1)
+    await_bytes(recv.at[0, others], row_recv.at[0])
+    pl.semaphore_signal(ready, inc=1, device_id=(my_row, flip(my_col, 1)), device_id_type=mesh_id)
     conv = convolve(short(0), 0)
 
-    for copy in edges:
-        copy.wait_recv()
-    line = lax.broadcasted_iota(jnp.int32, second.shape, 0)
-    above = jnp.where(my_row == 0, 0.0, edge_in[0, 0:1])
-    below = jnp.where(my_row == rows - 1, 0.0, edge_in[1, 0:1])
-    before = jnp.where(line == 0, above, pltpu.roll(second, 1, 0))
-    after = jnp.where(line == tok_rows - 1, below, pltpu.roll(second, tok_rows - 1, 0))
-    short_second = before * conv_ref[0, 2:3] + second * conv_ref[1, 2:3] + after * conv_ref[2, 2:3]
-    both = (short_second * (gate / (1.0 + jnp.exp(-gate)))).astype(low)
-    loads["perm"].wait()
-    both = jnp.dot(both, perm_ref[...], preferred_element_type=f32).astype(low)
-    per_group = rows * PACK
-    for g in range(groups):
-        gated[:, g] = both[:, g * per_group : (g + 1) * per_group].reshape(cols, width, per_group)
-    gate_copies = [
-        remote(
-            gated.at[flip(my_col, d)], gated_in.at[d], gate_send.at[d - 1], gate_recv.at[d - 1], my_row, flip(my_col, d)
-        )
-        for d in range(1, cols)
-    ]
-    for copy in gate_copies:
-        copy.start()
-    gated_in[0] = gated[my_col]
-
-    for copy in first_copies:
-        copy.wait_recv()
+    pass_on(0, ((1, 3), (2, 1)))
+    await_bytes(recv.at[1, others], row_recv.at[1])
     conv = convolve(short(1) * conv, 1)
 
     left = conv[:, :LANES].reshape(length_q, PACK, LANES)
@@ -627,54 +654,67 @@
             if dr == 0 and dc == 0:
                 continue
             row, col = flip(my_row, dr), flip(my_col, dc)
-            index = dr * cols + dc - 1
             piece_copies.append(
                 remote(
-                    piece.at[row * block_q + lax.div(col, 2), lax.rem(col, 2)], final.at[dc, my_row],
-                    piece_send.at[index], piece_recv.at[index], row, col,
+                    piece.at[row * block_q + lax.div(col, 2), lax.rem(col, 2)], final.at[dc * rows + my_row],
+                    piece_send, piece_recv, row, col,
                 )
             )
+    pl.semaphore_wait(ready, 1)
     for copy in piece_copies:
         copy.start()
-    final[0, my_row] = piece[my_row * block_q + lax.div(my_col, 2), lax.rem(my_col, 2)]
-
-    for key, copy in passed.items():
-        wide[key].wait_recv()
-        copy.start()
-        mates[key].start()
+    final[my_row] = piece[my_row * block_q + lax.div(my_col, 2), lax.rem(my_col, 2)]
+
+    pass_on(1, ((1, 2), (2, 0)))
+    await_bytes(weights.at[0, 0, 0], pass_recv.at[0])
+    for sub in (3, 1):
+        level_late[sub].start()
+        to_mate(3, sub, own_half, shared)
+    await_bytes(weights.at[0, 0], pass_recv.at[3])
+    for sub in (3, 1):
+        to_mate(3, sub, all_of, unshared)
+    await_bytes(weights.at[0, pl.ds(0, 2)], level_recv.at[0])
     for d in (1, 2):
-        level[d].wait_recv()
-        mates[d, 2 * d - 1].start()
-
-    for copy in gate_copies:
-        copy.wait_recv()
-    for copy in piece_copies:
-        copy.wait_recv()
+        to_mate(d, 2 * d - 1 - plane)
+    for index, sub in ((1, 2), (2, 0)):
+        await_bytes(weights.at[0, 0], pass_recv.at[index])
+        to_mate(3, sub)
+    await_bytes(weights.at[0, 0, 0], level_recv.at[1])
+    for sub in (3, 1):
+        to_mate(3, sub, far_half, shared)
+
+    await_bytes(gated_in.at[pl.ds(1, cols - 1)], gate_recv)
+    await_bytes(final.at[pl.ds(0, rows * cols - 1)], piece_recv)
     loads["w_out"].wait()
-    depth = weights.shape[4]
 
     def share(d):
-        outer = final[d].reshape(rows * PACK, LANES).astype(f32).T
+        outer = final[d * rows : (d + 1) * rows].reshape(rows * PACK, LANES).astype(f32).T
         outer = (outer * gated_in[d].reshape(groups * width, per_group).astype(f32)).astype(low)
         left = jnp.concatenate([outer[g * width : (g + 1) * width] for g in range(groups)], axis=1)
         right = jnp.concatenate([weights[d, :, g].reshape(per_group, depth) for g in range(groups)], axis=0)
         return jnp.dot(left, right, preferred_element_type=f32)
 
-    for d in (1, 2):
-        for sub in range(subs):
-            mates[d, sub].wait_recv()
+    await_bytes(weights.at[0], mate_recv.at[0])
     total[...] = share(0) + share(1) + share(2)
-    for d, sub in ((2, 0), (1, 2), (2, 1), (1, 3)):
-        passed[d, sub].wait_recv()
-        mates[3, sub].start()
-    for sub in range(subs):
-        mates[3, sub].wait_recv()
+    await_bytes(weights.at[0, pl.ds(0, subs)], mate_recv.at[1])
     out_ref[...] = (total[...] + share(3)).astype(low)
-    for copy in value_copies + first_copies + edges + gate_copies + piece_copies:
-        copy.wait_send()
-    for group in (wide, level, passed, mates):
-        for copy in group.values():
-            copy.wait_send()
+    for role in range(2):
+        await_bytes(send.at[role, others], row_send.at[role])
+
+    @pl.when(has_below)
+    def _():
+        await_bytes(edge_out.at[0], edge_send.at[0])
+
+    @pl.when(has_above)
+    def _():
+        await_bytes(edge_out.at[1], edge_send.at[1])
+
+    await_bytes(gated.at[pl.ds(1, cols - 1)], gate_send)
+    await_bytes(final.at[pl.ds(0, rows * cols - 1)], piece_send)
+    await_bytes(weights.at[0, pl.ds(0, 6)], wide_send)
+    await_bytes(weights.at[0, pl.ds(0, 5), 0], level_send)
+    await_bytes(weights.at[0, pl.ds(0, 7), 0], pass_send)
+    await_bytes(weights.at[pl.ds(0, 3), pl.ds(0, 4)], mate_send)
 
 
 def fast_body(
@@ -712,10 +752,13 @@
     w_rows = w_out.reshape(rows, groups, PACK, depth)
 
     first, last, twist, ahead, back = dft_tables(length)
+    size = groups * LANES
+    tables = jnp.asarray(
+        np.concatenate([first, last[:, :size], last[:, size:], ahead, back, perm]).astype(np.float32)
+    ).astype(jnp.bfloat16)
     operands = (
         flat, w_value, w_first, w_second, w_gate, w_rows, conv_taps, filter_embed, filter_freq.reshape(1, hid),
-        fproj, filter_decay, skip_gain, jnp.asarray(features), first, last, twist, ahead, back,
-        jnp.asarray(perm).astype(jnp.bfloat16),
+        fproj, filter_decay, skip_gain, jnp.asarray(features), tables, twist,
     )
     dma = pltpu.SemaphoreType.DMA
     f32, low = jnp.float32, jnp.bfloat16
@@ -735,12 +778,8 @@
             like(filter_decay),
             like(skip_gain),
             pltpu.VMEM(features.shape, low),
-            like(first),
-            like(last),
+            like(tables),
             like(twist),
-            like(ahead),
-            like(back),
-            pltpu.VMEM(perm.shape, low),
             pltpu.VMEM((2, rows, groups, block_q, PACK, LANES), low),
             pltpu.VMEM((2, rows, groups, block_q, PACK, LANES), low),
             pltpu.VMEM((2, 2, groups * half * PACK, LANES), f32),
@@ -752,26 +791,27 @@
             pltpu.VMEM((2, 8, chan_col), f32),
             pltpu.VMEM((2, 8, chan_col), f32),
             pltpu.VMEM((length_q, groups, PACK, LANES), low),
-            pltpu.VMEM((cols, rows, PACK, LANES), low),
+            pltpu.VMEM((cols * rows, PACK, LANES), low),
             pltpu.VMEM((cols, rows, groups, PACK, depth), low),
             pltpu.VMEM((width, depth), f32),
-            dma((len(operands),)),
-            dma((2, rows - 1)),
-            dma((2, rows - 1)),
+            dma((len(operands) - 3,)),
             dma((2,)),
             dma((2,)),
-            dma((cols - 1,)),
-            dma((cols - 1,)),
-            dma((rows * cols - 1,)),
-            dma((rows * cols - 1,)),
-            dma((6,)),
-            dma((6,)),
             dma((2,)),
             dma((2,)),
+            dma,
+            dma,
+            dma,
+            dma,
+            dma,
+            dma((3,)),
+            dma,
+            dma((2,)),
+            dma,
             dma((4,)),
-            dma((4,)),
-            dma(((cols - 1) * rows // 2,)),
-            dma(((cols - 1) * rows // 2,)),
+            dma,
+            dma((2,)),
+            pltpu.SemaphoreType.REGULAR,
             pltpu.SemaphoreType.REGULAR,
         ],
         compiler_params=pltpu.CompilerParams(

time: 27.4 us -> 24.9 us (0.909)
  Pallas kernels: 26.2 us -> 23.9 us
    pallas_call x1, Pallas kernels: 26.2 us -> 23.9 us  [fast_body(): pl.pallas_call(functools.partial(mixer_kernel, rows, cols, width, emb), o...]
where the time goes in v3:
time: 24.9 us; the launch traced here: 24.7 us
  Pallas kernels  23.9 us (96%)
  local copies, waits for them, and re-layouts  0.71 us (3%)
    pallas_call x1, Pallas kernels, fast_body(): pl.pallas_call(functools.partial(mixer_kernel, rows, cols, width, emb), o...  23.9 us
    unnamed x1, local copies, waits for them, and re-layouts  0.71 us

profile of v3, /device:TPU:0, one launch (start us, length us, event | category | flops | bytes accessed | tf_op | source)
XLA Modules:
  0.0 24.7 jit_solution(11284714350073892721)
XLA Ops:
  0.0 23.9 %shard_map.145 = bf16[64,2048]{1,0:T(8,128)(2,1)S(1)} custom-call(bf16[256,2048]{1,0:T(8,128)(2,1)} %bitcast.10, bf16[2048,256]{1,0:T(8,128)(2,1)} %w_value_hbm.1, bf16[2048,256]{1,0:T(8,128)(2,1)} %w_first_hbm.1, bf16[2048,256]{1,0:T(8,128)(2,1)} %w_second_hbm.1, bf16[2048,256]{1,0:T(8,128)(2,1)} %w_gate_hbm.1, bf16[8,2,16,2048]{3,2,1,0:T(8,128)(2,1)} %bitcast.11, ...), custom_call_target="tpu_custom_call" | custom-call | flops 12000000000 | bytes 8000000 | tf_op jit(solution)/shard_map/pallas_call | solution.py:766
  23.9 0.7 %copy.18 = bf16[1,64,2048]{2,1,0:T(8,128)(2,1)} copy(bf16[1,64,2048]{2,1,0:T(8,128)(2,1)S(1)} %bitcast.9) | data formatting | bytes 524288

commit v4 on v3

--- a/solution.py
+++ b/solution.py
@@ -262,9 +262,9 @@
     out_ref,
     tokens_ref, w_refs, conv_ref, embed_ref, freq_ref, fproj_ref, decay_ref, gain_ref, features_ref, tables_ref,
     twist_ref,
-    send, recv, spectra, taps_ref, stack_ref, coef_ref, gated, gated_in, edge_out, edge_in, piece, final, weights, total,
-    load_sem, row_send, row_recv, edge_send, edge_recv, gate_send, gate_recv, piece_send, piece_recv,
-    wide_send, wide_recv, level_send, level_recv, pass_send, pass_recv, mate_send, mate_recv, told, ready,
+    send, recv, spectra, taps_ref, stack_ref, coef_ref, gated, edge_out, edge_in, back_send, back_in, outer_send, outer_in, weights, total,
+    load_sem, row_send, row_recv, edge_send, edge_recv, piece_send, piece_recv, outer_sem,
+    wide_send, wide_recv, level_send, level_recv, pass_send, pass_recv, mate_send, mate_recv, told,
 ):
     my_row = lax.axis_index("row")
     my_col = lax.axis_index("col")
@@ -316,7 +316,10 @@
     def await_bytes(ref, sem):
         pltpu.make_async_copy(ref, ref, sem).wait()
 
-    token_sem, weight_sem = load_sem.at[0], load_sem.at[1]
+    token_sem, weight_sem, half_sem = load_sem.at[0], load_sem.at[1], load_sem.at[2]
+    half_rows = lambda half: pl.ds(half * (rows // 2), rows // 2)
+    own_rows = pltpu.make_async_copy(w_out_hbm.at[half_rows(side)], weights.at[0, half_rows(side)], half_sem)
+    own_rows.start()
     pltpu.make_async_copy(tokens_hbm, tokens_ref, token_sem).start()
     pltpu.make_async_copy(w_value_hbm, w_refs.at[0], token_sem).start()
     loads = {}
@@ -330,9 +333,9 @@
         ("features", features_hbm, features_ref),
         ("tables", tables_hbm, tables_ref),
         ("twist", twist_hbm, twist_ref),
-        ("w_out", w_out_hbm, weights.at[0]),
+        ("w_out", w_out_hbm.at[half_rows(1 - side)], weights.at[0, half_rows(1 - side)]),
     ):
-        loads[name] = pltpu.make_async_copy(src, dst, load_sem.at[2 + len(loads)])
+        loads[name] = pltpu.make_async_copy(src, dst, load_sem.at[3 + len(loads)])
     for role, w_hbm in ((2, w_second_hbm), (1, w_first_hbm), (3, w_gate_hbm)):
         pltpu.make_async_copy(w_hbm, w_refs.at[role], weight_sem).start()
     for copy in loads.values():
@@ -342,50 +345,43 @@
     subs = rows // 2
     row_of = lambda sub: side * subs + sub
 
-    def wide_copy(index, d, sub):
+    def wide_copy(group, d, sub):
         return remote(
-            w_out_hbm.at[row_of(sub)], weights.at[d, row_of(sub)],
-            wide_send, wide_recv.at[index // 2], my_row, flip(my_col, d),
+            weights.at[0, row_of(sub)], weights.at[d, row_of(sub)],
+            wide_send, wide_recv.at[group], my_row, flip(my_col, d),
         )
 
     wide = {
-        (d, sub): wide_copy(index, d, sub + plane if sub == mixed else sub)
-        for index, (d, sub, mixed) in enumerate(
-            ((1, 0, 0), (2, 2, 2), (1, 3, 0), (2, 1, 2), (1, 2, 0), (2, 0, 2))
-        )
+        (d, sub): wide_copy(group, d, sub + plane if group == 0 else sub)
+        for group, d, sub in ((0, 1, 0), (0, 2, 2), (1, 1, 3), (1, 2, 0), (2, 1, 2), (2, 2, 1))
     }
 
     def there(part, send_sem, recv_sem, row):
         return remote(part, part, send_sem, recv_sem, row, my_col)
 
-    own_half, far_half = pl.ds(plane, 1), pl.ds(1 - plane, 1)
-    all_of = pl.ds(0, groups)
-    level_row = flip(my_row, 2)
-    level = {
-        d: there(weights.at[d, row_of(2 * d - 2 + plane)], level_send, level_recv.at[0], level_row) for d in (1, 2)
-    }
-    level_late = {
-        sub: there(weights.at[3, row_of(sub), own_half, pl.ds(0, PACK), pl.ds(0, depth // 2)], level_send, level_recv.at[1], level_row) for sub in (3, 1)
-    }
-
-    shared, unshared = pl.ds(0, depth // 2), pl.ds(depth // 2, depth // 2)
-    every_row, every_lane = pl.ds(0, PACK), pl.ds(0, depth)
-
-    def pass_copy(index, d, sub, span, lanes):
+    levels = [
+        there(weights.at[d, row_of(2 * d - 2 + plane)], level_send, level_recv.at[d - 1], flip(my_row, 2)) for d in (1, 2)
+    ]
+    def pass_copy(index, d, sub):
         return remote(
-            weights.at[d, row_of(sub), span, every_row, lanes], weights.at[3, row_of(sub), span, every_row, lanes],
+            weights.at[d, row_of(sub)], weights.at[3, row_of(sub)],
             pass_send, pass_recv.at[index], my_row, flip(my_col, 3 - d),
         )
 
-    passed = {
-        (1, 3): [pass_copy(0, 1, 3, own_half, shared), pass_copy(3, 1, 3, all_of, unshared)],
-        (2, 1): [pass_copy(0, 2, 1, own_half, shared), pass_copy(3, 2, 1, all_of, unshared)],
-        (1, 2): [pass_copy(1, 1, 2, all_of, every_lane)],
-        (2, 0): [pass_copy(2, 2, 0, all_of, every_lane)],
-    }
-
-    def to_mate(d, sub, span=all_of, lanes=every_lane):
-        there(weights.at[d, row_of(sub), span, every_row, lanes], mate_send, mate_recv.at[d // 3], mate).start()
+    passed = {(d, sub): pass_copy(index, d, sub) for index, d, sub in ((0, 1, 3), (0, 2, 0), (1, 1, 2), (1, 2, 1))}
+
+    def to_mate(d, sub):
+        there(weights.at[d, row_of(sub)], mate_send, mate_recv.at[d // 3], mate).start()
+
+    def chunk(count):
+        return weights.at[0, pl.ds(0, count)]
+
+    def wide_arrived(group, keys):
+        await_bytes(chunk(len(keys)), wide_recv.at[group])
+        for d, sub in keys:
+            if (d, sub) in passed:
+                passed[d, sub].start()
+            to_mate(d, sub + plane if group == 0 else sub)
 
     far_first = sorted(range(1, rows), key=lambda d: -(d & (rows // 2)))
 
@@ -410,6 +406,7 @@
 
     value_copies, first_copies = row_copies(0), row_copies(1)
 
+    own_rows.wait()
     heard(0)
     for copy in wide.values():
         copy.start()
@@ -498,9 +495,9 @@
         taps_ref[od] = block.astype(low)
 
     size = LANES * groups
-    first_ref, last_ref, ahead_ref, back_ref, perm_ref = (
+    first_ref, last_ref, ahead_ref, back_ref = (
         tables_ref.at[pl.ds(start * size, count * size)]
-        for start, count in ((0, 2), (2, 2), (4, 1), (5, 1), (6, 1))
+        for start, count in ((0, 2), (2, 2), (4, 1), (5, 1))
     )
 
     def wide_twist(index):
@@ -575,10 +572,8 @@
                 spectra[order, 0] += spec[:, :LANES]
                 spectra[order, 1] -= spec[:, LANES:]
 
-    await_bytes(weights.at[0, pl.ds(0, 2)], wide_recv.at[0])
-    for d in (1, 2):
-        level[d].start()
-        to_mate(d, 2 * d - 2 + plane)
+    wide_arrived(0, ((1, 0), (2, 2)))
+    levels[0].start()
 
 
     @pl.when(has_above)
@@ -595,27 +590,9 @@
     before = jnp.where(line == 0, above, pltpu.roll(second, 1, 0))
     after = jnp.where(line == tok_rows - 1, below, pltpu.roll(second, tok_rows - 1, 0))
     short_second = before * conv_ref[0, 2:3] + second * conv_ref[1, 2:3] + after * conv_ref[2, 2:3]
-    both = (short_second * (gate / (1.0 + jnp.exp(-gate)))).astype(low)
-    both = jnp.dot(both, perm_ref[...], preferred_element_type=f32).astype(low)
-    per_group = rows * PACK
-    for g in range(groups):
-        gated[:, g] = both[:, g * per_group : (g + 1) * per_group].reshape(cols, width, per_group)
-    gate_copies = [
-        remote(
-            gated.at[flip(my_col, d)], gated_in.at[d], gate_send, gate_recv, my_row, flip(my_col, d)
-        )
-        for d in range(1, cols)
-    ]
-    for copy in gate_copies:
-        copy.start()
-    gated_in[0] = gated[my_col]
-
-    def pass_on(index, keys):
-        await_bytes(weights.at[0, pl.ds(0, 2)], wide_recv.at[1 + index])
-        for key in keys:
-            for copy in passed[key]:
-                copy.start()
-            to_mate(*key)
+    both = short_second * (gate / (1.0 + jnp.exp(-gate)))
+    for tile in range(halves):
+        gated[tile] = both[:, tile * LANES : (tile + 1) * LANES]
 
     def short(role):
         blocks = []
@@ -636,68 +613,69 @@
 
     others = pl.ds(0, rows - 1)
     await_bytes(recv.at[0, others], row_recv.at[0])
-    pl.semaphore_signal(ready, inc=1, device_id=(my_row, flip(my_col, 1)), device_id_type=mesh_id)
     conv = convolve(short(0), 0)
 
-    pass_on(0, ((1, 3), (2, 1)))
+    wide_arrived(1, ((1, 3), (2, 0)))
     await_bytes(recv.at[1, others], row_recv.at[1])
     conv = convolve(short(1) * conv, 1)
 
-    left = conv[:, :LANES].reshape(length_q, PACK, LANES)
-    right = conv[:, LANES:].reshape(length_q, PACK, LANES)
-    lane = lax.broadcasted_iota(jnp.int32, left.shape, 2)
-    piece[:, 0] = jnp.where(lane < width, left, pltpu.roll(right, width, 2)).astype(low)
-    piece[:, 1] = jnp.where(lane < width, pltpu.roll(left, width, 2), right).astype(low)
-    piece_copies = []
-    for dr in far_first + [0]:
-        for dc in range(cols):
-            if dr == 0 and dc == 0:
-                continue
-            row, col = flip(my_row, dr), flip(my_col, dc)
-            piece_copies.append(
-                remote(
-                    piece.at[row * block_q + lax.div(col, 2), lax.rem(col, 2)], final.at[dc * rows + my_row],
-                    piece_send, piece_recv, row, col,
-                )
-            )
-    pl.semaphore_wait(ready, 1)
-    for copy in piece_copies:
-        copy.start()
-    final[my_row] = piece[my_row * block_q + lax.div(my_col, 2), lax.rem(my_col, 2)]
-
-    pass_on(1, ((1, 2), (2, 0)))
-    await_bytes(weights.at[0, 0, 0], pass_recv.at[0])
-    for sub in (3, 1):
-        level_late[sub].start()
-        to_mate(3, sub, own_half, shared)
-    await_bytes(weights.at[0, 0], pass_recv.at[3])
-    for sub in (3, 1):
-        to_mate(3, sub, all_of, unshared)
-    await_bytes(weights.at[0, pl.ds(0, 2)], level_recv.at[0])
-    for d in (1, 2):
-        to_mate(d, 2 * d - 1 - plane)
-    for index, sub in ((1, 2), (2, 0)):
-        await_bytes(weights.at[0, 0], pass_recv.at[index])
-        to_mate(3, sub)
-    await_bytes(weights.at[0, 0, 0], level_recv.at[1])
-    for sub in (3, 1):
-        to_mate(3, sub, far_half, shared)
-
-    await_bytes(gated_in.at[pl.ds(1, cols - 1)], gate_recv)
-    await_bytes(final.at[pl.ds(0, rows * cols - 1)], piece_recv)
+    for g in range(groups):
+        back_send[:, :, g] = (
+            conv[:, g * LANES : (g + 1) * LANES].reshape(rows, block_q, PACK, LANES).astype(low)
+        )
+    for d in far_first:
+        peer = flip(my_row, d)
+        remote(back_send.at[peer], back_in.at[my_row], piece_send, piece_recv.at[2 * d // rows], peer, my_col).start()
+    levels[1].start()
+    back_in[my_row] = back_send[my_row]
+
+    wide_arrived(2, ((1, 2), (2, 1)))
+
+    per_tile = rows // halves
+    near_tile = lax.div(my_row, per_tile)
+
+    def finish(tile, far):
+        count = per_tile if far else per_tile - 1
+        await_bytes(back_in.at[pl.ds(0, count)], piece_recv.at[far])
+        for q in range(block_q):
+            block = back_in[pl.ds(tile * per_tile, per_tile), q].reshape(LANES, LANES).astype(f32).T
+            block = (block * gated[tile, q * LANES : (q + 1) * LANES]).astype(low)
+            spots = LANES // width
+            outer_send[far, q * spots : (q + 1) * spots] = block.reshape(spots, width, LANES)
+        for d in (3, 1, 2):
+            peer = flip(my_col, d)
+            remote(
+                outer_send.at[far, peer], outer_in.at[far, d], outer_sem.at[0], outer_sem.at[1 + far], my_row, peer
+            ).start()
+        outer_in[far, 0] = outer_send[far, my_col]
+
+    def share(tile, far):
+        await_bytes(outer_in.at[far, pl.ds(1, cols - 1)], outer_sem.at[1 + far])
+        left = jnp.concatenate([outer_in[far, d] for d in range(cols)], axis=1)
+        right = jnp.concatenate(
+            [weights[d, pl.ds(tile * per_tile, per_tile)].reshape(LANES, depth) for d in range(cols)], axis=0
+        )
+        return jnp.dot(left, right, preferred_element_type=f32)
+
+    finish(near_tile, 0)
+    await_bytes(chunk(2), pass_recv.at[0])
+    to_mate(3, 0)
+    to_mate(3, 3)
+    await_bytes(chunk(1), level_recv.at[0])
+    to_mate(1, 1 - plane)
+    finish(1 - near_tile, 1)
+    await_bytes(chunk(2), pass_recv.at[1])
+    to_mate(3, 2)
+    to_mate(3, 1)
+    await_bytes(chunk(1), level_recv.at[1])
+    to_mate(2, 3 - plane)
+
     loads["w_out"].wait()
-
-    def share(d):
-        outer = final[d * rows : (d + 1) * rows].reshape(rows * PACK, LANES).astype(f32).T
-        outer = (outer * gated_in[d].reshape(groups * width, per_group).astype(f32)).astype(low)
-        left = jnp.concatenate([outer[g * width : (g + 1) * width] for g in range(groups)], axis=1)
-        right = jnp.concatenate([weights[d, :, g].reshape(per_group, depth) for g in range(groups)], axis=0)
-        return jnp.dot(left, right, preferred_element_type=f32)
-
     await_bytes(weights.at[0], mate_recv.at[0])
-    total[...] = share(0) + share(1) + share(2)
-    await_bytes(weights.at[0, pl.ds(0, subs)], mate_recv.at[1])
-    out_ref[...] = (total[...] + share(3)).astype(low)
+    await_bytes(chunk(subs), mate_recv.at[1])
+    total[...] = share(near_tile, 0)
+    out_ref[...] = (total[...] + share(1 - near_tile, 1)).astype(low)
+
     for role in range(2):
         await_bytes(send.at[role, others], row_send.at[role])
 
@@ -709,11 +687,11 @@
     def _():
         await_bytes(edge_out.at[1], edge_send.at[1])
 
-    await_bytes(gated.at[pl.ds(1, cols - 1)], gate_send)
-    await_bytes(final.at[pl.ds(0, rows * cols - 1)], piece_send)
-    await_bytes(weights.at[0, pl.ds(0, 6)], wide_send)
-    await_bytes(weights.at[0, pl.ds(0, 5), 0], level_send)
-    await_bytes(weights.at[0, pl.ds(0, 7), 0], pass_send)
+    await_bytes(back_send.at[others], piece_send)
+    await_bytes(outer_send.at[pl.ds(0, 2), pl.ds(0, cols - 1)], outer_sem.at[0])
+    await_bytes(chunk(6), wide_send)
+    await_bytes(chunk(2), level_send)
+    await_bytes(chunk(4), pass_send)
     await_bytes(weights.at[pl.ds(0, 3), pl.ds(0, 4)], mate_send)
 
 
@@ -744,9 +722,6 @@
     features = np.concatenate([features, np.zeros((emb_pad - emb, length))]).astype(np.float32).astype(np.float64)
     high, middle, least = host_split(features)
     features = np.concatenate([high, middle, high, least, middle, high]).astype(jnp.bfloat16.dtype)
-    own = np.arange(chan_col).reshape(rows, groups, PACK).transpose(1, 0, 2).reshape(-1)
-    perm = np.zeros((chan_col, chan_col), np.float32)
-    perm[own, np.arange(chan_col)] = 1.0
     lanes = chan_col // LANES
     fproj = filter_proj.reshape(hid, 2, 2, lanes, LANES).transpose(0, 1, 3, 2, 4).reshape(hid * 4 * lanes, LANES)
     w_rows = w_out.reshape(rows, groups, PACK, depth)
@@ -754,7 +729,7 @@
     first, last, twist, ahead, back = dft_tables(length)
     size = groups * LANES
     tables = jnp.asarray(
-        np.concatenate([first, last[:, :size], last[:, size:], ahead, back, perm]).astype(np.float32)
+        np.concatenate([first, last[:, :size], last[:, size:], ahead, back]).astype(np.float32)
     ).astype(jnp.bfloat16)
     operands = (
         flat, w_value, w_first, w_second, w_gate, w_rows, conv_taps, filter_embed, filter_freq.reshape(1, hid),
@@ -786,32 +761,31 @@
             pltpu.VMEM((4, chans, length), low),
             pltpu.VMEM((16, chan_col), f32),
             pltpu.VMEM((8, groups, PACK, LANES), f32),
-            pltpu.VMEM((cols, groups, width, rows * PACK), low),
-            pltpu.VMEM((cols, groups, width, rows * PACK), low),
+            pltpu.VMEM((lanes, tok_rows, LANES), f32),
             pltpu.VMEM((2, 8, chan_col), f32),
             pltpu.VMEM((2, 8, chan_col), f32),
-            pltpu.VMEM((length_q, groups, PACK, LANES), low),
-            pltpu.VMEM((cols * rows, PACK, LANES), low),
+            pltpu.VMEM((rows, block_q, groups, PACK, LANES), low),
+            pltpu.VMEM((rows, block_q, groups, PACK, LANES), low),
+            pltpu.VMEM((2, cols, width, LANES), low),
+            pltpu.VMEM((2, cols, width, LANES), low),
             pltpu.VMEM((cols, rows, groups, PACK, depth), low),
             pltpu.VMEM((width, depth), f32),
-            dma((len(operands) - 3,)),
+            dma((len(operands) - 2,)),
             dma((2,)),
             dma((2,)),
             dma((2,)),
             dma((2,)),
             dma,
-            dma,
-            dma,
-            dma,
+            dma((2,)),
+            dma((3,)),
             dma,
             dma((3,)),
             dma,
             dma((2,)),
             dma,
-            dma((4,)),
+            dma((2,)),
             dma,
             dma((2,)),
-            pltpu.SemaphoreType.REGULAR,
             pltpu.SemaphoreType.REGULAR,
         ],
         compiler_params=pltpu.CompilerParams(

time: 24.9 us -> 23.8 us (0.956)
  Pallas kernels: 23.9 us -> 23 us
    pallas_call x1, Pallas kernels: 23.9 us -> 23 us  [fast_body(): pl.pallas_call(functools.partial(mixer_kernel, rows, cols, width, emb), o...]
where the time goes in v4:
time: 23.8 us; the launch traced here: 23.7 us
  Pallas kernels  23 us (97%)
  local copies, waits for them, and re-layouts  0.71 us (3%)
    pallas_call x1, Pallas kernels, fast_body(): pl.pallas_call(functools.partial(mixer_kernel, rows, cols, width, emb), o...  23 us
    unnamed x1, local copies, waits for them, and re-layouts  0.71 us

profile of v4, /device:TPU:0, one launch (start us, length us, event | category | flops | bytes accessed | tf_op | source)
XLA Modules:
  0.0 23.7 jit_solution(17914436789354409997)
XLA Ops:
  0.0 23.0 %shard_map.145 = bf16[64,2048]{1,0:T(8,128)(2,1)S(1)} custom-call(bf16[256,2048]{1,0:T(8,128)(2,1)} %bitcast.10, bf16[2048,256]{1,0:T(8,128)(2,1)} %w_value_hbm.1, bf16[2048,256]{1,0:T(8,128)(2,1)} %w_first_hbm.1, bf16[2048,256]{1,0:T(8,128)(2,1)} %w_second_hbm.1, bf16[2048,256]{1,0:T(8,128)(2,1)} %w_gate_hbm.1, bf16[8,2,16,2048]{3,2,1,0:T(8,128)(2,1)} %bitcast.11, ...), custom_call_target="tpu_custom_call" | custom-call | flops 12000000000 | bytes 8000000 | tf_op jit(solution)/shard_map/pallas_call | solution.py:741
  23.0 0.7 %copy.18 = bf16[1,64,2048]{2,1,0:T(8,128)(2,1)} copy(bf16[1,64,2048]{2,1,0:T(8,128)(2,1)S(1)} %bitcast.9) | data formatting | bytes 524288

commit v5 on v4

--- a/solution.py
+++ b/solution.py
@@ -359,9 +359,17 @@
     def there(part, send_sem, recv_sem, row):
         return remote(part, part, send_sem, recv_sem, row, my_col)
 
-    levels = [
-        there(weights.at[d, row_of(2 * d - 2 + plane)], level_send, level_recv.at[d - 1], flip(my_row, 2)) for d in (1, 2)
+    def level_copy(index, d, group, start, count):
+        part = weights.at[d, row_of(2 * d - 2 + plane), group, pl.ds(0, PACK), pl.ds(start, count)]
+        return there(part, level_send, level_recv.at[index], flip(my_row, 2))
+
+    ahead_of = depth // 2
+    early = [level_copy(0, 1, pl.ds(0, groups), 0, depth), level_copy(1, 2, pl.ds(0, 1), 0, ahead_of)]
+    late = [
+        level_copy(1, 2, pl.ds(0, 1), ahead_of, depth - ahead_of),
+        level_copy(1, 2, pl.ds(1, groups - 1), 0, depth),
     ]
+
     def pass_copy(index, d, sub):
         return remote(
             weights.at[d, row_of(sub)], weights.at[3, row_of(sub)],
@@ -406,8 +414,8 @@
 
     value_copies, first_copies = row_copies(0), row_copies(1)
 
+    heard(0)
     own_rows.wait()
-    heard(0)
     for copy in wide.values():
         copy.start()
     await_bytes(w_refs.at[pl.ds(0, 2)], token_sem)
@@ -573,7 +581,8 @@
                 spectra[order, 1] -= spec[:, LANES:]
 
     wide_arrived(0, ((1, 0), (2, 2)))
-    levels[0].start()
+    for copy in early:
+        copy.start()
 
 
     @pl.when(has_above)
@@ -626,7 +635,8 @@
     for d in far_first:
         peer = flip(my_row, d)
         remote(back_send.at[peer], back_in.at[my_row], piece_send, piece_recv.at[2 * d // rows], peer, my_col).start()
-    levels[1].start()
+    for copy in late:
+        copy.start()
     back_in[my_row] = back_send[my_row]
 
     wide_arrived(2, ((1, 2), (2, 1)))

time: 23.8 us -> 23.8 us (level)
  no operation moved by 1% of the time
where the time goes in v5:
time: 23.8 us; the launch traced here: 23.7 us
  Pallas kernels  23 us (97%)
  local copies, waits for them, and re-layouts  0.71 us (3%)
    pallas_call x1, Pallas kernels, fast_body(): pl.pallas_call(functools.partial(mixer_kernel, rows, cols, width, emb), o...  23 us
    unnamed x1, local copies, waits for them, and re-layouts  0.71 us

profile of v5, /device:TPU:0, one launch (start us, length us, event | category | flops | bytes accessed | tf_op | source)
XLA Modules:
  0.0 23.7 jit_solution(8492698886030906440)
XLA Ops:
  0.0 23.0 %shard_map.145 = bf16[64,2048]{1,0:T(8,128)(2,1)S(1)} custom-call(bf16[256,2048]{1,0:T(8,128)(2,1)} %bitcast.10, bf16[2048,256]{1,0:T(8,128)(2,1)} %w_value_hbm.1, bf16[2048,256]{1,0:T(8,128)(2,1)} %w_first_hbm.1, bf16[2048,256]{1,0:T(8,128)(2,1)} %w_second_hbm.1, bf16[2048,256]{1,0:T(8,128)(2,1)} %w_gate_hbm.1, bf16[8,2,16,2048]{3,2,1,0:T(8,128)(2,1)} %bitcast.11, ...), custom_call_target="tpu_custom_call" | custom-call | flops 12000000000 | bytes 8000000 | tf_op jit(solution)/shard_map/pallas_call | solution.py:751
  23.0 0.7 %copy.18 = bf16[1,64,2048]{2,1,0:T(8,128)(2,1)} copy(bf16[1,64,2048]{2,1,0:T(8,128)(2,1)S(1)} %bitcast.9) | data formatting | bytes 524288

commit v6 on v5

--- a/solution.py
+++ b/solution.py
@@ -426,6 +426,10 @@
     recv[0, my_row] = send[0, my_row]
 
     await_bytes(w_refs.at[pl.ds(1, 3)], weight_sem)
+    project_turned(1)
+    for copy in first_copies:
+        copy.start()
+    recv[1, my_row] = send[1, my_row]
     second = project(2).astype(low).astype(f32)
     edge_out[0] = jnp.broadcast_to(second[tok_rows - 1 :], edge_out.shape[1:])
     edge_out[1] = jnp.broadcast_to(second[:1], edge_out.shape[1:])
@@ -442,10 +446,6 @@
     def _():
         edge_copy(1, -1).start()
 
-    project_turned(1)
-    for copy in first_copies:
-        copy.start()
-    recv[1, my_row] = send[1, my_row]
     gate = project(3).astype(low).astype(f32)
     loads["conv"].wait()
 
@@ -584,25 +584,6 @@
     for copy in early:
         copy.start()
 
-
-    @pl.when(has_above)
-    def _():
-        await_bytes(edge_in.at[0], edge_recv.at[0])
-
-    @pl.when(has_below)
-    def _():
-        await_bytes(edge_in.at[1], edge_recv.at[1])
-
-    line = lax.broadcasted_iota(jnp.int32, second.shape, 0)
-    above = jnp.where(has_above, edge_in[0, 0:1], 0.0)
-    below = jnp.where(has_below, edge_in[1, 0:1], 0.0)
-    before = jnp.where(line == 0, above, pltpu.roll(second, 1, 0))
-    after = jnp.where(line == tok_rows - 1, below, pltpu.roll(second, tok_rows - 1, 0))
-    short_second = before * conv_ref[0, 2:3] + second * conv_ref[1, 2:3] + after * conv_ref[2, 2:3]
-    both = short_second * (gate / (1.0 + jnp.exp(-gate)))
-    for tile in range(halves):
-        gated[tile] = both[:, tile * LANES : (tile + 1) * LANES]
-
     def short(role):
         blocks = []
         for g in range(groups):
@@ -640,6 +621,26 @@
     back_in[my_row] = back_send[my_row]
 
     wide_arrived(2, ((1, 2), (2, 1)))
+
+
+    @pl.when(has_above)
+    def _():
+        await_bytes(edge_in.at[0], edge_recv.at[0])
+
+    @pl.when(has_below)
+    def _():
+        await_bytes(edge_in.at[1], edge_recv.at[1])
+
+    line = lax.broadcasted_iota(jnp.int32, second.shape, 0)
+    above = jnp.where(has_above, edge_in[0, 0:1], 0.0)
+    below = jnp.where(has_below, edge_in[1, 0:1], 0.0)
+    before = jnp.where(line == 0, above, pltpu.roll(second, 1, 0))
+    after = jnp.where(line == tok_rows - 1, below, pltpu.roll(second, tok_rows - 1, 0))
+    short_second = before * conv_ref[0, 2:3] + second * conv_ref[1, 2:3] + after * conv_ref[2, 2:3]
+    both = short_second * (gate / (1.0 + jnp.exp(-gate)))
+    for tile in range(halves):
+        gated[tile] = both[:, tile * LANES : (tile + 1) * LANES]
+
 
     per_tile = rows // halves
     near_tile = lax.div(my_row, per_tile)

time: 23.8 us -> 23.8 us (level)
  no operation moved by 1% of the time
where the time goes in v6:
time: 23.8 us; the launch traced here: 23.7 us
  Pallas kernels  23 us (97%)
  local copies, waits for them, and re-layouts  0.71 us (3%)
    pallas_call x1, Pallas kernels, fast_body(): pl.pallas_call(functools.partial(mixer_kernel, rows, cols, width, emb), o...  23 us
    unnamed x1, local copies, waits for them, and re-layouts  0.71 us

profile of v6, /device:TPU:0, one launch (start us, length us, event | category | flops | bytes accessed | tf_op | source)
XLA Modules:
  0.0 23.7 jit_solution(5310587818348897157)
XLA Ops:
  0.0 23.0 %shard_map.145 = bf16[64,2048]{1,0:T(8,128)(2,1)S(1)} custom-call(bf16[256,2048]{1,0:T(8,128)(2,1)} %bitcast.10, bf16[2048,256]{1,0:T(8,128)(2,1)} %w_value_hbm.1, bf16[2048,256]{1,0:T(8,128)(2,1)} %w_first_hbm.1, bf16[2048,256]{1,0:T(8,128)(2,1)} %w_second_hbm.1, bf16[2048,256]{1,0:T(8,128)(2,1)} %w_gate_hbm.1, bf16[8,2,16,2048]{3,2,1,0:T(8,128)(2,1)} %bitcast.11, ...), custom_call_target="tpu_custom_call" | custom-call | flops 12000000000 | bytes 8000000 | tf_op jit(solution)/shard_map/pallas_call | solution.py:752
  23.0 0.7 %copy.18 = bf16[1,64,2048]{2,1,0:T(8,128)(2,1)} copy(bf16[1,64,2048]{2,1,0:T(8,128)(2,1)S(1)} %bitcast.9) | data formatting | bytes 524288
